TPU v7x, 32 devices: a whole 2x2x4 slice. The times are simulated.
32 devices in a mesh: ep: 8 (over z, y), tp: 4 (over x, core).
Axes of the slice: x: 2, y: 2, z: 4, core: 2. Of those that a mesh axis runs over, the one named last changes fastest.
Arguments:
- tokens: bfloat16 [128, 2048], P('ep'), may hold values from -6 to 6
- norm_gain: bfloat16 [2048], replicated, may hold values from 0.099609375 to 1.8984375
- query_weight: bfloat16 [2048, 1024], P('ep', 'tp'), may hold values from -0.125 to 0.125
- key_weight: bfloat16 [2048, 1024], P('ep', 'tp'), may hold values from -0.125 to 0.125
- value_weight: bfloat16 [2048, 2048], P('ep', 'tp'), may hold values from -0.125 to 0.125
- outgate_weight: bfloat16 [2048, 2048], P('ep', 'tp'), may hold values from -0.125 to 0.125
- beta_weight: bfloat16 [2048, 16], replicated, may hold values from -0.125 to 0.125
- decay_weight: bfloat16 [2048, 16], replicated, may hold values from -0.125 to 0.125
- decay_rate: float32 [16], P('tp'), may hold values from 0.02 to 6
- decay_bias: float32 [16], P('tp'), may hold values from -3 to 3
- head_gain: bfloat16 [128], replicated, may hold values from 0.099609375 to 1.8984375
- recurrent: float32 [128, 16, 128, 128], P('ep', 'tp'), may hold values from -3 to 3
- output_weight: bfloat16 [2048, 2048], P('tp', 'ep'), may hold values from -0.125 to 0.125
- ffn_gain: bfloat16 [2048], replicated, may hold values from 0.099609375 to 1.8984375
- routes: int32 [128, 4], P('ep'), may hold values from 0 to 7, all different within a row; in each aligned block of 16 rows (0 to 15, 16 to 31, ...) at most 16 rows name the same one
- route_weight: float32 [128, 4], P('ep'), may hold values from 0.1 to 1
- expert_gate: bfloat16 [8, 2048, 512], P('ep', None, 'tp'), may hold values from -0.125 to 0.125
- expert_up: bfloat16 [8, 2048, 512], P('ep', None, 'tp'), may hold values from -0.125 to 0.125
- expert_down: bfloat16 [8, 512, 2048], P('ep', 'tp'), may hold values from -0.25 to 0.25
- shared_gate: bfloat16 [2048, 512], P('ep', 'tp'), may hold values from -0.125 to 0.125
- shared_up: bfloat16 [2048, 512], P('ep', 'tp'), may hold values from -0.125 to 0.125
- shared_down: bfloat16 [512, 2048], P('tp', 'ep'), may hold values from -0.25 to 0.25
- branch_gate: bfloat16 [2048], replicated, may hold values from -0.125 to 0.125
Outputs:
- layer_out: bfloat16 [128, 2048], P('ep')
- new_state: float32 [128, 16, 128, 128], P('ep', 'tp')
Inputs may be any that keep to these rules, and one draw needn't show every extreme that they name: `routes`: each row names 4 different experts. Among the rows of one aligned block of 16 rows no expert is named more than 16 times, and some block reaches it: one expert is named exactly 16 times there.
All inputs are finite; a program needn't handle non-finite values.
Results may differ from a plain program's by a relative error of at most 0.019.
Values may be sent and summed in bfloat16 or wider, within the bound.
A program may use at most 64 MiB of HBM per device.

v0:
```python
import functools

import jax
import jax.numpy as jnp
from jax import lax
from jax.experimental import pallas as pl
from jax.experimental.pallas import tpu as pltpu
from jax.sharding import PartitionSpec as P

EPS = 1e-06
ROUTED_SCALE = 2.5
MESH = pl.DeviceIdType.MESH
F32 = jnp.float32
BF16 = jnp.bfloat16
STEP = 4


def silu(v):
    return v / (1.0 + jnp.exp(-v))


def sigmoid(v):
    return 1.0 / (1.0 + jnp.exp(-v))


def rms_scale(values, gain):
    values = values.astype(F32)
    return (
        values
        * lax.rsqrt(jnp.mean(values * values, axis=-1, keepdims=True) + EPS)
        * gain.astype(F32).reshape(1, -1)
    )


def unit_rows(values):
    return values * lax.rsqrt(jnp.sum(values * values, axis=-1, keepdims=True) + EPS)


def dot_nt(a, b):
    return lax.dot_general(a, b, (((1,), (1,)), ((), ())), preferred_element_type=F32)


def remote(src, dst, send_sem, recv_sem, e, t):
    return pltpu.make_async_remote_copy(
        src_ref=src,
        dst_ref=dst,
        send_sem=send_sem,
        recv_sem=recv_sem,
        device_id=(e, t),
        device_id_type=MESH,
    )


def loop(lo, hi, body):
    def step(i, c):
        body(i)
        return c

    lax.fori_loop(lo, hi, step, 0)


def project_kernel(
    n,
    key_dim,
    tokens_ref,
    gain_ref,
    qw_ref,
    kw_ref,
    vw_ref,
    gw_ref,
    beta_ref,
    decay_ref,
    rate_ref,
    bias_ref,
    routes_ref,
    rw_ref,
    kq_ref,
    value_ref,
    gate_ref,
    scalars_ref,
    route_ref,
    weights,
    xsend,
    xbuf,
    pbuf,
    rbuf,
    wsem,
    xs,
    xr,
    ps,
    pr,
):
    me, tp = lax.axis_index("ep"), lax.axis_index("tp")
    rows = tokens_ref.shape[0]
    qc, vc = qw_ref.shape[1], vw_ref.shape[1]
    total = 2 * qc + 2 * vc
    depth = qw_ref.shape[0]
    fetches = []
    at = 0
    for i, w in enumerate((qw_ref, kw_ref, vw_ref, gw_ref)):
        c = pltpu.make_async_copy(w, weights.at[:, pl.ds(at, w.shape[1])], wsem.at[i])
        c.start()
        fetches.append(c)
        at += w.shape[1]

    barrier = pltpu.get_barrier_semaphore()

    def greet(i):
        pl.semaphore_signal(
            barrier, inc=1, device_id=(lax.rem(me + i, n), tp), device_id_type=MESH
        )

    loop(1, n, greet)

    normed = rms_scale(tokens_ref[...], gain_ref[...]).astype(BF16)
    for e in range(n):
        xsend[e] = normed[:, e * depth : (e + 1) * depth]
    pl.semaphore_wait(barrier, n - 1)

    def send_x(i):
        p = lax.rem(me + i, n)
        remote(xsend.at[p], xbuf.at[me], xs.at[i], xr.at[me], p, tp).start()

    loop(1, n, send_x)
    xbuf[me] = xsend[me]

    heads = rate_ref.shape[1]
    column = lax.broadcasted_iota(jnp.int32, (rows, beta_ref.shape[0]), 1)
    lane = lax.broadcasted_iota(jnp.int32, (rows, heads), 1)

    def own_heads(w):
        logits = dot_nt(normed, w)
        own = jnp.zeros((rows, heads), F32)
        for h in range(heads):
            kept = jnp.where(column == tp * heads + h, logits, 0.0)
            own = jnp.where(lane == h, jnp.sum(kept, axis=1, keepdims=True), own)
        return own

    strength = sigmoid(own_heads(beta_ref[...]))
    shifted = own_heads(decay_ref[...]) + bias_ref[...]
    softplus = jnp.maximum(shifted, 0.0) + jnp.log1p(jnp.exp(-jnp.abs(shifted)))
    retain = jnp.exp(-rate_ref[...] * softplus)
    rw = rw_ref[...]
    scaled = rw / jnp.sum(rw, axis=0, keepdims=True) * ROUTED_SCALE
    routes = routes_ref[...]
    expert = lax.broadcasted_iota(jnp.int32, (128, rows), 0)
    by_expert = jnp.zeros((128, rows), F32)
    for k in range(routes.shape[0]):
        by_expert = by_expert + jnp.where(
            expert == routes[k : k + 1, :], scaled[k : k + 1, :], 0.0
        )
    by_expert = by_expert.T
    lane = lax.broadcasted_iota(jnp.int32, (rows, 128), 1)
    for e in range(n):
        w = by_expert[:, e : e + 1]
        high = w.astype(BF16).astype(F32)
        pbuf[e, :, total:] = jnp.where(lane < 64, high, w - high).astype(BF16)

    for c in fetches:
        c.wait()

    def got_x(i):
        p = lax.rem(me + i, n)
        remote(xbuf.at[p], xbuf.at[p], xs.at[i], xr.at[p], p, tp).wait_recv()

    loop(1, n, got_x)
    x = xbuf[...].reshape(n * rows, depth)
    part = 512
    for c in range(0, total, part):
        width = min(part, total - c)
        out = jnp.dot(x, weights[:, c : c + width], preferred_element_type=F32)
        pbuf[:, :, c : c + width] = out.astype(BF16).reshape(n, rows, width)

    def send_p(i):
        p = lax.rem(me + i, n)
        remote(pbuf.at[p], rbuf.at[me], ps.at[i], pr.at[me], p, tp).start()

    loop(1, n, send_p)
    rbuf[me] = pbuf[me]

    def got_p(i):
        p = lax.rem(me + i, n)
        remote(rbuf.at[p], rbuf.at[p], ps.at[i], pr.at[p], p, tp).wait_recv()

    loop(1, n, got_p)

    def gathered(c, width):
        acc = rbuf[0, :, c : c + width].astype(F32)
        for e in range(1, n):
            acc = acc + rbuf[e, :, c : c + width].astype(F32)
        return acc.astype(BF16).astype(F32)

    keys = qc // key_dim
    q_rows = [
        unit_rows(silu(gathered(j * key_dim, key_dim))) * key_dim ** (-0.5)
        for j in range(keys)
    ]
    k_rows = [unit_rows(silu(gathered(qc + j * key_dim, key_dim))) for j in range(keys)]
    for j in range(0, vc, 128):
        value_ref[:, j : j + 128] = silu(gathered(2 * qc + j, 128))
        gate_ref[:, j : j + 128] = silu(gathered(2 * qc + vc + j, 128))
    stacked = q_rows + k_rows
    stacked.append(jnp.zeros((128 - 2 * keys * rows, key_dim), F32))
    kq_ref[...] = jnp.concatenate(stacked, axis=0).T
    lane = lax.broadcasted_iota(jnp.int32, scalars_ref.shape, 1)
    scalars = jnp.zeros(scalars_ref.shape, F32)
    for h in range(heads):
        scalars = jnp.where(lane == h, retain[:, h : h + 1], scalars)
        scalars = jnp.where(lane == heads + h, strength[:, h : h + 1], scalars)
    for j in range(keys):
        qk = jnp.sum(q_rows[j] * k_rows[j], axis=1, keepdims=True)
        scalars = jnp.where(lane == 2 * heads + j, qk, scalars)
    scalars_ref[...] = scalars
    for e in range(n):
        w = rbuf[e, :, total:].astype(F32)
        route_ref[e * rows : (e + 1) * rows, :] = jnp.broadcast_to(
            w[:, 0:1] + w[:, 64:65], (rows, 128)
        )

    def sent(i):
        p = lax.rem(me + i, n)
        remote(xsend.at[p], xbuf.at[me], xs.at[i], xr.at[me], p, tp).wait_send()
        remote(pbuf.at[p], rbuf.at[me], ps.at[i], pr.at[me], p, tp).wait_send()

    loop(1, n, sent)


def delta_kernel(
    keys, rows, scalars_ref, kq_ref, value_ref, state_ref, new_ref, read_ref, held
):
    g = pl.program_id(0)
    heads = state_ref.shape[1]
    key_dim, value_dim = state_ref.shape[2], state_ref.shape[3]
    turned = pltpu.roll(kq_ref[...], lax.rem(128 - STEP * g, 128), 1)
    values = pltpu.roll(value_ref[...], lax.rem(rows - STEP * g, rows), 0)
    for i in range(STEP):
        s = STEP * g + i
        for j in range(keys):
            q = jnp.broadcast_to(
                turned[:, j * rows + i : j * rows + i + 1], (key_dim, value_dim)
            )
            at = (keys + j) * rows + i
            k = jnp.broadcast_to(turned[:, at : at + 1], (key_dim, value_dim))
            qk = scalars_ref[s, 2 * heads + j]
            for h in range(j * (heads // keys), (j + 1) * (heads // keys)):
                cols = slice(h * value_dim, (h + 1) * value_dim)
                retain, strength = scalars_ref[s, h], scalars_ref[s, heads + h]
                decayed = state_ref[i, h] * retain
                predicted = jnp.sum(decayed * k, axis=0, keepdims=True)
                before = jnp.sum(decayed * q, axis=0, keepdims=True)
                correction = strength * (values[i : i + 1, cols] - predicted)
                new_ref[i, h] = decayed + k * correction
                held[i : i + 1, cols] = before + qk * correction
    row = lax.broadcasted_iota(jnp.int32, held.shape, 0)
    mine = (row >= STEP * g) & (row < STEP * (g + 1))
    read_ref[...] = jnp.where(mine, pltpu.roll(held[...], STEP * g, 0), read_ref[...])


def mix_kernel(
    n,
    m,
    read_ref,
    gate_ref,
    head_gain_ref,
    tokens_ref,
    ow_ref,
    ffn_gain_ref,
    eg_ref,
    eu_ref,
    ed_ref,
    sg_ref,
    su_ref,
    sd_ref,
    branch_ref,
    route_ref,
    out_ref,
    ow,
    eg,
    eu,
    ed,
    hbuf,
    mbuf,
    mrecv,
    ssend,
    sbuf,
    sdown,
    resid,
    fbuf,
    pbuf,
    srecv,
    rsend,
    rrecv,
    obuf,
    wsem,
    hs,
    hr,
    ms,
    mr,
    ss,
    sr,
    fs,
    fr,
    gs,
    gr,
    bs,
    br,
    rs,
    rr,
    os_,
    or_,
):
    me, tp = lax.axis_index("ep"), lax.axis_index("tp")
    count = n * m
    lin = me * m + tp
    half = m // 2
    core = lax.rem(tp, 2)
    pair = tp + 1 - 2 * core
    rows, width = tokens_ref.shape
    fetches = []
    split = width // 2
    moves = [(ow_ref, ow), (eg_ref, eg), (eu_ref, eu)]
    moves += [(ed_ref.at[0, :, pl.ds(c * split, split)], ed.at[c]) for c in range(2)]
    for i, (w, v) in enumerate(moves):
        c = pltpu.make_async_copy(w, v, wsem.at[i])
        c.start()
        fetches.append(c)

    barrier = pltpu.get_barrier_semaphore()

    def greet(i):
        p = lax.rem(lin + i, count)
        pl.semaphore_signal(
            barrier, inc=1, device_id=(p // m, lax.rem(p, m)), device_id_type=MESH
        )

    loop(1, count, greet)

    value_dim = head_gain_ref.shape[0]
    for h in range(0, read_ref.shape[1], value_dim):
        cols = slice(h, h + value_dim)
        hbuf[me, :, cols] = (
            rms_scale(read_ref[:, cols], head_gain_ref[...]) * gate_ref[:, cols]
        ).astype(BF16)
    pl.semaphore_wait(barrier, count - 1)

    def send_h(i):
        p = lax.rem(me + i, n)
        remote(hbuf.at[me], hbuf.at[me], hs.at[i], hr.at[me], p, tp).start()

    loop(1, n, send_h)
    units = ssend.shape[1] // 3
    for at, w in enumerate((sg_ref, su_ref, sd_ref)):
        by_unit = w[...] if at == 2 else w[...].astype(F32).T.astype(BF16)
        for e in range(n):
            ssend[e, at * units : (at + 1) * units] = by_unit[e * units : (e + 1) * units]
    fetches[0].wait()

    def got_h(i):
        p = lax.rem(me + i, n)
        remote(hbuf.at[p], hbuf.at[p], hs.at[i], hr.at[p], p, tp).wait_recv()

    loop(1, n, got_h)
    h_all = hbuf[...].reshape(n * rows, hbuf.shape[2])
    block = ow.shape[1]
    mbuf[...] = (
        jnp.dot(h_all, ow[...], preferred_element_type=F32).astype(BF16).reshape(n, rows, block)
    )

    def send_m(i):
        p = lax.rem(lin + i, count)
        e, t = p // m, lax.rem(p, m)
        remote(mbuf.at[e], mrecv.at[lin], ms.at[i], mr.at[lin], e, t).start()

    loop(1, count, send_m)
    mrecv[lin] = mbuf[me]

    def send_s(i):
        p = lax.rem(me + i, n)
        remote(ssend.at[p], sbuf.at[me], ss.at[i], sr.at[me], p, tp).start()

    loop(1, n, send_s)
    sbuf[me] = ssend[me]

    def got_m(i):
        p = lax.rem(lin + i, count)
        e, t = p // m, lax.rem(p, m)
        remote(mrecv.at[p], mrecv.at[p], ms.at[i], mr.at[p], e, t).wait_recv()

    loop(1, count, got_m)
    pieces = []
    for e in range(n):
        acc = mrecv[e * m].astype(F32)
        for t in range(1, m):
            acc = acc + mrecv[e * m + t].astype(F32)
        pieces.append(acc)
    mix = jnp.concatenate(pieces, axis=1)
    residual = (tokens_ref[...].astype(F32) + mix).astype(BF16).astype(F32)
    quarter = width // m
    for t in range(m):
        resid[t] = residual[:, t * quarter : (t + 1) * quarter]
    ffn_in = rms_scale(residual, ffn_gain_ref[...]).astype(BF16)
    fbuf[0, me] = ffn_in[:, :split]
    fbuf[1, me] = ffn_in[:, split:]

    def send_f(i):
        p = lax.rem(me + i, n)
        remote(
            fbuf.at[core, me], fbuf.at[core, me], fs.at[i], fr.at[core, me], p, tp
        ).start()

    loop(1, n, send_f)

    def pass_f(i):
        p = lax.rem(me + n - i, n)
        mine = fbuf.at[core, p]
        remote(mine, mine, fs.at[i], fr.at[core, p], p, tp).wait_recv()
        remote(mine, mine, gs.at[i], gr.at[p], me, pair).start()

    loop(1, n, pass_f)

    def got_s(i):
        p = lax.rem(me + i, n)
        remote(sbuf.at[p], sbuf.at[p], ss.at[i], sr.at[p], p, tp).wait_recv()

    loop(1, n, got_s)
    shared = jnp.concatenate([sbuf[e] for e in range(n)], axis=1)
    for c in range(2):
        sdown[c] = shared[2 * units :, c * split : (c + 1) * split]
    for c in fetches[1:]:
        c.wait()

    def got_f(i):
        p = lax.rem(me + n - i, n)
        other = fbuf.at[1 - core, p]
        remote(other, other, gs.at[i], gr.at[p], me, pair).wait_recv()

    loop(1, n, got_f)

    x0 = fbuf[0].reshape(n * rows, split)
    x1 = fbuf[1].reshape(n * rows, split)

    def up(w):
        return jnp.dot(x0, w[0, :split], preferred_element_type=F32) + jnp.dot(
            x1, w[0, split:], preferred_element_type=F32
        )

    def up_shared(w):
        return dot_nt(x0, w[:, :split]) + dot_nt(x1, w[:, split:])

    act = (silu(up(eg)) * up(eu)).astype(BF16)
    shared_act = (
        silu(up_shared(shared[:units])) * up_shared(shared[units : 2 * units])
    ).astype(BF16)
    bg = branch_ref[...].astype(F32).reshape(1, -1)
    branch = sigmoid(
        jnp.sum(x0.astype(F32) * bg[:, :split], axis=1, keepdims=True)
        + jnp.sum(x1.astype(F32) * bg[:, split:], axis=1, keepdims=True)
    )
    weight = route_ref[:, 0:1]

    def down(c):
        out = weight * jnp.dot(act, ed[c], preferred_element_type=F32)
        out = out + branch * jnp.dot(shared_act, sdown[c], preferred_element_type=F32)
        pbuf[c] = out.astype(BF16)

    down(1 - core)
    swap = remote(pbuf.at[1 - core], srecv, bs.at[0], br.at[0], me, pair)
    swap.start()
    down(core)
    swap.wait_recv()
    for e in range(n):
        these = slice(e * rows, (e + 1) * rows)
        both = pbuf[core, these].astype(F32) + srecv[these].astype(F32)
        for x in range(half):
            rsend[e * half + x] = both[:, x * quarter : (x + 1) * quarter].astype(BF16)

    blocks = n * half
    mine = me * half + tp // 2

    def send_r(i):
        p = lax.rem(mine + i, blocks)
        e, x = p // half, lax.rem(p, half)
        remote(rsend.at[p], rrecv.at[mine], rs.at[i], rr.at[mine], e, 2 * x + core).start()

    loop(1, blocks, send_r)
    rrecv[mine] = rsend[mine]

    def got_r(i):
        p = lax.rem(mine + i, blocks)
        e, x = p // half, lax.rem(p, half)
        remote(rrecv.at[p], rrecv.at[p], rs.at[i], rr.at[p], e, 2 * x + core).wait_recv()

    loop(1, blocks, got_r)
    place = core * half + tp // 2
    acc = resid[place]
    for p in range(blocks):
        acc = acc + rrecv[p].astype(F32)
    obuf[place] = acc.astype(BF16)

    def send_o(i):
        t = lax.rem(tp + i, m)
        remote(obuf.at[place], obuf.at[place], os_.at[i], or_.at[place], me, t).start()

    loop(1, m, send_o)

    def got_o(i):
        t = lax.rem(tp + i, m)
        there = lax.rem(t, 2) * half + t // 2
        remote(obuf.at[there], obuf.at[there], os_.at[i], or_.at[there], me, t).wait_recv()

    loop(1, m, got_o)
    for t in range(m):
        out_ref[:, t * quarter : (t + 1) * quarter] = obuf[t]

    def sent_ep(i):
        p = lax.rem(me + i, n)
        remote(hbuf.at[me], hbuf.at[me], hs.at[i], hr.at[me], p, tp).wait_send()
        remote(ssend.at[p], sbuf.at[me], ss.at[i], sr.at[me], p, tp).wait_send()
        remote(
            fbuf.at[core, me], fbuf.at[core, me], fs.at[i], fr.at[core, me], p, tp
        ).wait_send()
        b = lax.rem(me + n - i, n)
        remote(fbuf.at[core, b], fbuf.at[core, b], gs.at[i], gr.at[b], me, pair).wait_send()

    loop(1, n, sent_ep)

    def sent_m(i):
        p = lax.rem(lin + i, count)
        e, t = p // m, lax.rem(p, m)
        remote(mbuf.at[e], mrecv.at[lin], ms.at[i], mr.at[lin], e, t).wait_send()

    loop(1, count, sent_m)
    swap.wait_send()

    def sent_r(i):
        p = lax.rem(mine + i, blocks)
        e, x = p // half, lax.rem(p, half)
        remote(
            rsend.at[p], rrecv.at[mine], rs.at[i], rr.at[mine], e, 2 * x + core
        ).wait_send()

    loop(1, blocks, sent_r)

    def sent_o(i):
        t = lax.rem(tp + i, m)
        remote(obuf.at[place], obuf.at[place], os_.at[i], or_.at[place], me, t).wait_send()

    loop(1, m, sent_o)


VMEM = pl.BlockSpec(memory_space=pltpu.VMEM)
ANY = pl.BlockSpec(memory_space=pl.ANY)


def per_device(
    n,
    m,
    tokens,
    norm_gain,
    query_weight,
    key_weight,
    value_weight,
    outgate_weight,
    beta_weight,
    decay_weight,
    decay_rate,
    decay_bias,
    head_gain,
    recurrent,
    output_weight,
    ffn_gain,
    routes,
    route_weight,
    expert_gate,
    expert_up,
    expert_down,
    shared_gate,
    shared_up,
    shared_down,
    branch_gate,
):
    rows, width = tokens.shape
    _, heads, key_dim, value_dim = recurrent.shape
    depth, qc = query_weight.shape
    vc = value_weight.shape[1]
    keys = qc // key_dim
    total = 2 * qc + 2 * vc
    sds = jax.ShapeDtypeStruct
    dma = pltpu.SemaphoreType.DMA
    units = shared_gate.shape[1] // n
    cols = shared_down.shape[1]
    kq, value, gate, scalars, route = pl.pallas_call(
        functools.partial(project_kernel, n, key_dim),
        out_shape=(
            sds((key_dim, 128), F32),
            sds((rows, vc), F32),
            sds((rows, vc), F32),
            sds((rows, 2 * heads + keys), F32),
            sds((n * rows, 128), F32),
        ),
        in_specs=[VMEM] * 2 + [ANY] * 4 + [VMEM] * 6,
        out_specs=(VMEM,) * 5,
        scratch_shapes=[
            pltpu.VMEM((depth, total), BF16),
            pltpu.VMEM((n, rows, depth), BF16),
            pltpu.VMEM((n, rows, depth), BF16),
            pltpu.VMEM((n, rows, total + 128), BF16),
            pltpu.VMEM((n, rows, total + 128), BF16),
            dma((4,)),
            dma((n,)),
            dma((n,)),
            dma((n,)),
            dma((n,)),
        ],
        compiler_params=pltpu.CompilerParams(collective_id=0, has_side_effects=True),
    )(
        tokens,
        norm_gain,
        query_weight,
        key_weight,
        value_weight,
        outgate_weight,
        beta_weight.T,
        decay_weight.T,
        decay_rate[None, :],
        decay_bias[None, :],
        routes.T,
        route_weight.T,
    )

    new_state, readout = pl.pallas_call(
        functools.partial(delta_kernel, keys, rows),
        out_shape=(sds(recurrent.shape, F32), sds((rows, vc), F32)),
        grid=(rows // STEP,),
        in_specs=[
            pl.BlockSpec(memory_space=pltpu.SMEM),
            pl.BlockSpec((key_dim, 128), lambda g: (0, 0)),
            pl.BlockSpec((rows, vc), lambda g: (0, 0)),
            pl.BlockSpec((STEP, heads, key_dim, value_dim), lambda g: (g, 0, 0, 0)),
        ],
        out_specs=(
            pl.BlockSpec((STEP, heads, key_dim, value_dim), lambda g: (g, 0, 0, 0)),
            pl.BlockSpec((rows, vc), lambda g: (0, 0)),
        ),
        scratch_shapes=[pltpu.VMEM((rows, vc), F32)],
        compiler_params=pltpu.CompilerParams(dimension_semantics=("arbitrary",)),
    )(scalars, kq, value, recurrent)

    quarter = width // m
    blocks = n * (m // 2)
    layer_out = pl.pallas_call(
        functools.partial(mix_kernel, n, m),
        out_shape=sds((rows, width), BF16),
        in_specs=[VMEM] * 4 + [ANY, VMEM] + [ANY] * 3 + [VMEM] * 5,
        out_specs=VMEM,
        scratch_shapes=[
            pltpu.VMEM(output_weight.shape, BF16),
            pltpu.VMEM(expert_gate.shape, BF16),
            pltpu.VMEM(expert_up.shape, BF16),
            pltpu.VMEM((2, expert_down.shape[1], width // 2), BF16),
            pltpu.VMEM((n, rows, vc), BF16),
            pltpu.VMEM((n, rows, cols), BF16),
            pltpu.VMEM((n * m, rows, cols), BF16),
            pltpu.VMEM((n, 3 * units, cols), BF16),
            pltpu.VMEM((n, 3 * units, cols), BF16),
            pltpu.VMEM((2, units, width // 2), BF16),
            pltpu.VMEM((m, rows, quarter), F32),
            pltpu.VMEM((2, n, rows, width // 2), BF16),
            pltpu.VMEM((2, n * rows, width // 2), BF16),
            pltpu.VMEM((n * rows, width // 2), BF16),
            pltpu.VMEM((blocks, rows, quarter), BF16),
            pltpu.VMEM((blocks, rows, quarter), BF16),
            pltpu.VMEM((m, rows, quarter), BF16),
            dma((5,)),
            dma((n,)),
            dma((n,)),
            dma((n * m,)),
            dma((n * m,)),
            dma((n,)),
            dma((n,)),
            dma((n,)),
            dma((2, n)),
            dma((n,)),
            dma((n,)),
            dma((1,)),
            dma((1,)),
            dma((blocks,)),
            dma((blocks,)),
            dma((m,)),
            dma((m,)),
        ],
        compiler_params=pltpu.CompilerParams(collective_id=1, has_side_effects=True),
    )(
        readout,
        gate,
        head_gain,
        tokens,
        output_weight,
        ffn_gain,
        expert_gate,
        expert_up,
        expert_down,
        shared_gate,
        shared_up,
        shared_down,
        branch_gate,
        route,
    )
    return (layer_out, new_state)


def solution(mesh):
    return jax.shard_map(
        functools.partial(per_device, mesh.shape["ep"], mesh.shape["tp"]),
        mesh=mesh,
        in_specs=(
            P("ep", None),
            P(),
            P("ep", "tp"),
            P("ep", "tp"),
            P("ep", "tp"),
            P("ep", "tp"),
            P(),
            P(),
            P("tp"),
            P("tp"),
            P(),
            P("ep", "tp", None, None),
            P("tp", "ep"),
            P(),
            P("ep", None),
            P("ep", None),
            P("ep", None, "tp"),
            P("ep", None, "tp"),
            P("ep", "tp", None),
            P("ep", "tp"),
            P("ep", "tp"),
            P("tp", "ep"),
            P(),
        ),
        out_specs=(P("ep", None), P("ep", "tp", None, None)),
        check_vma=False,
    )
```

profile of v0, /device:TPU:0, one launch (start us, length us, event | category | flops | bytes accessed | tf_op | source)
XLA Modules:
  0.0 71.5 jit_solution(16150858039371960007)
XLA Ops:
  0.6 20.8 %shard_map.230 = (f32[128,128]{1,0:T(8,128)}, f32[16,512]{1,0:T(8,128)}, f32[16,512]{1,0:T(8,128)}, f32[16,10]{1,0:T(8,128)}, f32[128,128]{1,0:T(8,128)}) custom-call(bf16[16,2048]{1,0:T(8,128)(2,1)} %tokens_ref.3, bf16[2048]{0:T(1024)(128)(2,1)} %gain_ref.1, bf16[256,256]{1,0:T(8,128)(2,1)} %qw_ref.1, bf16[256,256]{1,0:T(8,128)(2,1)} %kw_ref.1, ...), custom_call_target="tpu_custom_call" | custom-call | tf_op jit(solution)/shard_map/pallas_call | solution.py:592
  21.4 5.7 %shard_map.231 = (f32[16,4,128,128]{3,2,1,0:T(8,128)}, f32[16,512]{1,0:T(8,128)}) custom-call(f32[16,10]{1,0:T(8,128)} %get-tuple-element.9.scalars_ref, f32[128,128]{1,0:T(8,128)} %get-tuple-element.10.kq_ref, f32[16,512]{1,0:T(8,128)} %get-tuple-element.11.value_ref, f32[16,4,128,128]{3,2,1,0:T(8,128)} %state_ref.1), custom_call_target="tpu_custom_call" | custom-call | tf_op jit(solution)/shard_map/pallas_call | solution.py:631
  27.1 42.9 %shard_map.232 = bf16[16,2048]{1,0:T(8,128)(2,1)} custom-call(f32[16,512]{1,0:T(8,128)} %get-tuple-element.12.read_ref, f32[16,512]{1,0:T(8,128)} %get-tuple-element.13.gate_ref, bf16[128]{0:T(256)(128)(2,1)} %head_gain_ref.1, bf16[16,2048]{1,0:T(8,128)(2,1)} %tokens_ref.3, bf16[512,256]{1,0:T(8,128)(2,1)} %ow_ref.1, bf16[2048]{0:T(1024)(128)(2,1)} %ffn_gain_ref.1, ...), custom_call_target="tpu_custom_call" | custom-call | tf_op jit(solution)/shard_map/pallas_call | solution.py:651
  70.0 1.5 %copy.26 = bf16[16,2048]{1,0:T(8,128)(2,1)} copy(bf16[16,2048]{1,0:T(8,128)(2,1)} %shard_map.232) | data formatting | bytes 131072
where the time goes:
time: 71.9 us; the launch traced here: 71.5 us
  Pallas kernels  69.4 us (97%)
  local copies, waits for them, and re-layouts  1.47 us (2%)
    pallas_call x1, Pallas kernels, per_device(): pl.pallas_call(functools.partial(mix_kernel, n, m), out_shape=sds((rows,...  42.9 us
    pallas_call x1, Pallas kernels, per_device(): pl.pallas_call(functools.partial(project_kernel, n, key_dim), out_shape=(...  20.8 us
    pallas_call x1, Pallas kernels, per_device(): pl.pallas_call(functools.partial(delta_kernel, keys, rows), out_shape=(sd...  5.7 us
    unnamed x1, local copies, waits for them, and re-layouts  1.47 us

commit v1 on v0

v1 whole, which is shorter than its diff:
```python
import functools
import types

import jax
import jax.numpy as jnp
from jax import lax
from jax.experimental import pallas as pl
from jax.experimental.pallas import tpu as pltpu
from jax.sharding import PartitionSpec as P

EPS = 1e-06
ROUTED_SCALE = 2.5
MESH = pl.DeviceIdType.MESH
F32 = jnp.float32
BF16 = jnp.bfloat16
STATE_PARTS = 4


def silu(v):
    return v / (1.0 + jnp.exp(-v))


def sigmoid(v):
    return 1.0 / (1.0 + jnp.exp(-v))


def rms_scale(values, gain):
    values = values.astype(F32)
    return (
        values
        * lax.rsqrt(jnp.mean(values * values, axis=-1, keepdims=True) + EPS)
        * gain.astype(F32).reshape(1, -1)
    )


def unit_rows(values):
    return values * lax.rsqrt(jnp.sum(values * values, axis=-1, keepdims=True) + EPS)


def dot(a, b):
    return jnp.dot(a, b, preferred_element_type=F32)


def dot_nt(a, b):
    return lax.dot_general(a, b, (((1,), (1,)), ((), ())), preferred_element_type=F32)


def remote(src, dst, send_sem, recv_sem, e, t):
    return pltpu.make_async_remote_copy(
        src_ref=src,
        dst_ref=dst,
        send_sem=send_sem,
        recv_sem=recv_sem,
        device_id=(e, t),
        device_id_type=MESH,
    )


def loop(lo, hi, body):
    def step(i, c):
        body(i)
        return c

    lax.fori_loop(lo, hi, step, 0)


def layer_kernel(n, m, names, *refs):
    r = types.SimpleNamespace(**dict(zip(names, refs)))
    me, tp = lax.axis_index("ep"), lax.axis_index("tp")
    count = n * m
    lin = me * m + tp
    half = m // 2
    group = n // m
    core = lax.rem(tp, 2)
    pair = tp + 1 - 2 * core
    xi = tp // 2
    rows, width = r.tokens.shape
    depth, qc = r.qw_hbm.shape
    vc = r.vw_hbm.shape[1]
    key_dim, value_dim = r.new.shape[2], r.new.shape[3]
    heads = r.new.shape[1]
    keys = qc // key_dim
    near = 2 * qc + vc
    cols = r.ow.shape[1]
    hidden = r.eg_hbm.shape[2]
    quarter = width // m
    units = r.ssend.shape[1] // 3
    mates = half * group
    tall = mates * rows

    fetches = {}

    def fetch(name, src, dst):
        c = pltpu.make_async_copy(src, dst, r.wsem.at[len(fetches)])
        c.start()
        fetches[name] = c

    for name in ("tokens", "gain", "sg", "su", "sd", "beta", "decay", "rate", "bias"):
        fetch(name, getattr(r, name + "_hbm"), getattr(r, name))
    at = 0
    for name in ("qw", "kw", "vw", "gw"):
        src = getattr(r, name + "_hbm")
        fetch(name, src, r.weights.at[:, pl.ds(at, src.shape[1])])
        at += src.shape[1]
    for name in ("routes", "rw", "head_gain", "ffn_gain", "bg"):
        fetch(name, getattr(r, name + "_hbm"), getattr(r, name))
    part = rows // STATE_PARTS
    for i in range(STATE_PARTS):
        these = pl.ds(i * part, part)
        fetch(("state", i), r.state_hbm.at[these], r.new.at[these])
    fetch("ow", r.ow_hbm, r.ow)
    mine = pl.ds(pl.multiple_of(core * hidden, hidden), hidden)
    fetch("eg", r.eg_hbm.at[0], r.eg.at[:, mine])
    fetch("eu", r.eu_hbm.at[0], r.eu.at[:, mine])
    fetch("ed", r.ed_hbm.at[0], r.ed.at[mine])

    barrier = pltpu.get_barrier_semaphore()

    def greet(i):
        p = lax.rem(lin + i, count)
        pl.semaphore_signal(
            barrier, inc=1, device_id=(p // m, lax.rem(p, m)), device_id_type=MESH
        )

    loop(1, count, greet)

    fetches["tokens"].wait()
    fetches["gain"].wait()
    tokens = r.tokens[...]
    normed = rms_scale(tokens, r.gain[...]).astype(BF16)
    for e in range(n):
        r.xsend[e] = normed[:, e * depth : (e + 1) * depth]
        r.tsend[e] = tokens[:, e * depth : (e + 1) * depth]
    for at, name in enumerate(("sg", "su", "sd")):
        fetches[name].wait()
        w = getattr(r, name)[...]
        by_unit = w if at == 2 else w.astype(F32).T.astype(BF16)
        for e in range(n):
            r.ssend[e, at * units : (at + 1) * units] = by_unit[e * units : (e + 1) * units]
    pl.semaphore_wait(barrier, count - 1)

    def x_copy(i):
        p = lax.rem(me + i, n)
        return remote(r.xsend.at[p], r.xbuf.at[me], r.xs.at[i], r.xr.at[me], p, tp)

    loop(1, n, lambda i: x_copy(i).start())
    r.xbuf[me] = r.xsend[me]

    def s_copy(i):
        p = lax.rem(me + i, n)
        return remote(r.ssend.at[p], r.sbuf.at[core, me], r.ss.at[i], r.sr.at[me], p, tp)

    loop(1, n, lambda i: s_copy(i).start())
    r.sbuf[core, me] = r.ssend[me]

    e_copies = [
        remote(r.eg_hbm.at[0], r.eg.at[:, mine], r.es.at[0], r.er.at[0], me, pair),
        remote(r.eu_hbm.at[0], r.eu.at[:, mine], r.es.at[1], r.er.at[1], me, pair),
        remote(r.ed_hbm.at[0], r.ed.at[mine], r.es.at[2], r.er.at[2], me, pair),
    ]
    for c in e_copies:
        c.start()

    for name in ("beta", "decay", "rate", "bias", "routes", "rw"):
        fetches[name].wait()
    column = lax.broadcasted_iota(jnp.int32, (rows, r.beta.shape[0]), 1)

    def own_heads(w):
        logits = dot_nt(normed, w)
        return [
            jnp.sum(jnp.where(column == tp * heads + h, logits, 0.0), axis=1, keepdims=True)
            for h in range(heads)
        ]

    def wide(v):
        return jnp.broadcast_to(v, (rows, value_dim))

    beta = own_heads(r.beta[...])
    decay = own_heads(r.decay[...])
    strengths = []
    for h in range(heads):
        at = slice(h * value_dim, (h + 1) * value_dim)
        strength = sigmoid(wide(beta[h]))
        shifted = wide(decay[h]) + r.bias[:, h : h + 1]
        softplus = jnp.maximum(shifted, 0.0) + jnp.log1p(jnp.exp(-jnp.abs(shifted)))
        retain = jnp.exp(-r.rate[:, h : h + 1] * softplus)
        r.retain[:, at] = retain
        r.pull[:, at] = strength * retain
        strengths.append(strength)
    rw = r.rw[...]
    scaled = rw / jnp.sum(rw, axis=0, keepdims=True) * ROUTED_SCALE
    routes = r.routes[...]
    expert = lax.broadcasted_iota(jnp.int32, (128, rows), 0)
    by_expert = jnp.zeros((128, rows), F32)
    for k in range(routes.shape[0]):
        by_expert = by_expert + jnp.where(
            expert == routes[k : k + 1, :], scaled[k : k + 1, :], 0.0
        )
    by_expert = by_expert.T
    lane = lax.broadcasted_iota(jnp.int32, (rows, 128), 1)
    for e in range(n):
        w = by_expert[:, e : e + 1]
        high = w.astype(BF16).astype(F32)
        r.bsend[e, :, vc:] = jnp.where(lane < 64, high, w - high).astype(BF16)

    for name in ("qw", "kw", "vw", "gw"):
        fetches[name].wait()

    def got_x(i):
        p = lax.rem(me + i, n)
        remote(r.xbuf.at[p], r.xbuf.at[p], r.xs.at[i], r.xr.at[p], p, tp).wait_recv()

    loop(1, n, got_x)
    x = r.xbuf[...].reshape(n * rows, depth)

    def project(lo, hi, to):
        step = 512
        for c in range(lo, hi, step):
            size = min(step, hi - c)
            out = dot(x, r.weights[:, c : c + size])
            to[:, :, c - lo : c - lo + size] = out.astype(BF16).reshape(n, rows, size)

    def a_copy(i):
        p = lax.rem(me + i, n)
        return remote(r.asend.at[p], r.abuf.at[me], r.as_.at[i], r.ar.at[me], p, tp)

    def b_copy(i):
        p = lax.rem(me + i, n)
        return remote(r.bsend.at[p], r.bbuf.at[me], r.bs.at[i], r.br.at[me], p, tp)

    project(0, near, r.asend)
    loop(1, n, lambda i: a_copy(i).start())
    project(near, near + vc, r.bsend)
    loop(1, n, lambda i: b_copy(i).start())
    r.abuf[me] = r.asend[me]
    r.bbuf[me] = r.bsend[me]

    def t_copy(i):
        p = lax.rem(me + i, n)
        at = lax.rem(me, group)
        return remote(r.tsend.at[p], r.tbuf.at[at], r.ts.at[i], r.tr.at[at], p, tp)

    @pl.when(tp == me // group)
    def _():
        loop(1, n, lambda i: t_copy(i).start())
        r.tbuf[lax.rem(me, group)] = r.tsend[me]

    def s_pass(i):
        p = lax.rem(me + i, n)
        ref = r.sbuf.at[core, p]
        return remote(ref, ref, r.s2s.at[i], r.s2r.at[p], me, pair)

    def got_s(i):
        p = lax.rem(me + i, n)
        ref = r.sbuf.at[core, p]
        remote(ref, ref, r.ss.at[i], r.sr.at[p], p, tp).wait_recv()
        s_pass(i).start()

    s_pass(0).start()
    loop(1, n, got_s)

    def got_a(i):
        p = lax.rem(me + i, n)
        remote(r.abuf.at[p], r.abuf.at[p], r.as_.at[i], r.ar.at[p], p, tp).wait_recv()

    loop(1, n, got_a)

    def gathered(ref, c, size):
        acc = ref[0, :, c : c + size].astype(F32)
        for e in range(1, n):
            acc = acc + ref[e, :, c : c + size].astype(F32)
        return acc.astype(BF16).astype(F32)

    q_rows = [
        unit_rows(silu(gathered(r.abuf, j * key_dim, key_dim))) * key_dim ** (-0.5)
        for j in range(keys)
    ]
    k_rows = [
        unit_rows(silu(gathered(r.abuf, qc + j * key_dim, key_dim))) for j in range(keys)
    ]
    for h in range(heads):
        at = slice(h * value_dim, (h + 1) * value_dim)
        r.push[:, at] = strengths[h] * silu(
            gathered(r.abuf, 2 * qc + h * value_dim, value_dim)
        )
    for j in range(keys):
        r.qk[:, j * value_dim : (j + 1) * value_dim] = wide(
            jnp.sum(q_rows[j] * k_rows[j], axis=1, keepdims=True)
        )
    stacked = q_rows + k_rows
    stacked.append(jnp.zeros((128 - 2 * keys * rows, key_dim), F32))
    r.kq[...] = jnp.concatenate(stacked, axis=0).T
    for i in range(STATE_PARTS):
        fetches[("state", i)].wait()
    fetches["head_gain"].wait()

    share = heads // keys

    def h_copy(j, i):
        p = lax.rem(me + i, n)
        ref = r.hbuf.at[j, me]
        return remote(ref, ref, r.hs.at[j, i], r.hr.at[j, me], p, tp)

    def got_b(i):
        p = lax.rem(me + i, n)
        remote(r.bbuf.at[p], r.bbuf.at[p], r.bs.at[i], r.br.at[p], p, tp).wait_recv()

    for j in range(keys):

        for s in range(rows):
            q = jnp.broadcast_to(r.kq[:, j * rows + s : j * rows + s + 1], (key_dim, value_dim))
            at = (keys + j) * rows + s
            k = jnp.broadcast_to(r.kq[:, at : at + 1], (key_dim, value_dim))
            one = slice(s, s + 1)
            qk = r.qk[one, j * value_dim : (j + 1) * value_dim]
            for h in range(j * share, (j + 1) * share):
                c = slice(h * value_dim, (h + 1) * value_dim)
                state = r.new[s, h]
                retain = r.retain[one, c]
                predicted = jnp.sum(state * k, axis=0, keepdims=True)
                before = jnp.sum(state * q, axis=0, keepdims=True)
                correction = r.push[one, c] - r.pull[one, c] * predicted
                r.new[s, h] = state * retain + k * correction
                r.held[one, c] = before * retain + qk * correction

        if j == 0:
            loop(1, n, got_b)
        for h in range(j * share, (j + 1) * share):
            c = slice(h * value_dim, (h + 1) * value_dim)
            at = (h - j * share) * value_dim
            gate = silu(gathered(r.bbuf, h * value_dim, value_dim))
            r.hbuf[j, me, :, at : at + value_dim] = (
                rms_scale(r.held[:, c], r.head_gain[...]) * gate
            ).astype(BF16)
        loop(1, n, functools.partial(lambda j, i: h_copy(j, i).start(), j))

    for a in range(half):
        for b in range(group):
            e = (2 * a + core) * group + b
            w = r.bbuf[e, :, vc:].astype(F32)
            at = (a * group + b) * rows
            r.routed[at : at + rows] = jnp.broadcast_to(
                w[:, 0:1] + w[:, 64:65], (rows, 128)
            )

    def got_s2(i):
        p = lax.rem(me + i, n)
        ref = r.sbuf.at[1 - core, p]
        remote(ref, ref, r.s2s.at[i], r.s2r.at[p], me, pair).wait_recv()

    loop(0, n, got_s2)
    for c in range(2):
        r.shared[c] = jnp.concatenate([r.sbuf[c, e] for e in range(n)], axis=1)
    fetches["ow"].wait()

    def got_h(j, i):
        p = lax.rem(me + i, n)
        ref = r.hbuf.at[j, p]
        remote(ref, ref, r.hs.at[j, i], r.hr.at[j, p], p, tp).wait_recv()

    chunk = share * value_dim
    mix = None
    for j in range(keys):
        loop(1, n, functools.partial(got_h, j))
        term = dot(r.hbuf[j].reshape(n * rows, chunk), r.ow[j * chunk : (j + 1) * chunk])
        mix = term if mix is None else mix + term
    r.msend[...] = mix.astype(BF16).reshape(m, group * rows, cols)

    def m_copy(i):
        t = lax.rem(tp + i, m)
        return remote(r.msend.at[t], r.mbuf.at[tp], r.ms.at[i], r.mr.at[tp], me, t)

    loop(1, m, lambda i: m_copy(i).start())
    r.mbuf[tp] = r.msend[tp]

    def got_t(a):
        e = tp * group + a

        @pl.when(e != me)
        def _():
            remote(r.tbuf.at[a], r.tbuf.at[a], r.ts.at[0], r.tr.at[a], e, tp).wait_recv()

    loop(0, group, got_t)

    def got_m(i):
        t = lax.rem(tp + i, m)
        remote(r.mbuf.at[t], r.mbuf.at[t], r.ms.at[i], r.mr.at[t], me, t).wait_recv()

    loop(1, m, got_m)
    acc = r.mbuf[0].astype(F32)
    for t in range(1, m):
        acc = acc + r.mbuf[t].astype(F32)
    residual = (r.tbuf[...].reshape(group * rows, cols).astype(F32) + acc).astype(BF16)
    r.resid[xi, me] = residual.reshape(group, rows, cols)

    def f_copy(i):
        p = lax.rem(me + i, n)
        ref = r.resid.at[xi, me]
        return remote(ref, ref, r.fs.at[i], r.fr.at[me], p, tp)

    def f_pass(i, k):
        p = lax.rem(me + n - i, n)
        ref = r.resid.at[xi, p]
        t = 2 * lax.rem(xi + k, half) + core
        return remote(ref, ref, r.gs.at[k, i], r.gr.at[xi, p], me, t)

    loop(1, n, lambda i: f_copy(i).start())
    for k in range(1, half):
        f_pass(0, k).start()

    def got_f(i):
        p = lax.rem(me + n - i, n)
        ref = r.resid.at[xi, p]
        remote(ref, ref, r.fs.at[i], r.fr.at[p], p, tp).wait_recv()
        for k in range(1, half):
            f_pass(i, k).start()

    loop(1, n, got_f)
    for name in ("ffn_gain", "bg", "eg", "eu", "ed"):
        fetches[name].wait()
    for i, ref in enumerate((r.eg.at[:, pl.ds(pl.multiple_of((1 - core) * hidden, hidden), hidden)],
                             r.eu.at[:, pl.ds(pl.multiple_of((1 - core) * hidden, hidden), hidden)],
                             r.ed.at[pl.ds(pl.multiple_of((1 - core) * hidden, hidden), hidden)])):
        remote(ref, ref, r.es.at[i], r.er.at[i], me, pair).wait_recv()

    def got_g(i):
        p = lax.rem(me + n - i, n)
        for k in range(1, half):
            a = lax.rem(xi + k, half)
            ref = r.resid.at[a, p]
            remote(ref, ref, r.gs.at[k, i], r.gr.at[a, p], me, 2 * a + core).wait_recv()

    loop(0, n, got_g)

    owner = me // group
    held_here = core == lax.rem(owner, 2)
    place, which = owner // 2, lax.rem(me, group)

    def d_copy():
        return remote(
            r.resid.at[place, pl.ds(pair * group, group), which],
            r.rown,
            r.ds.at[0],
            r.dr.at[0],
            me,
            pair,
        )

    @pl.when(held_here)
    def _():
        d_copy().start()
        r.rown[...] = r.resid[place, pl.ds(tp * group, group), which]

    blocks = [r.resid[:, e].reshape(tall, cols).astype(F32) for e in range(n)]
    square = blocks[0] * blocks[0]
    for b in blocks[1:]:
        square = square + b * b
    scale = lax.rsqrt(jnp.sum(square, axis=1, keepdims=True) / width + EPS)
    gain = r.ffn_gain[...].astype(F32).reshape(1, -1)
    ffn = jnp.concatenate(
        [
            (b * scale * gain[:, e * cols : (e + 1) * cols]).astype(BF16)
            for e, b in enumerate(blocks)
        ],
        axis=1,
    )
    act = (silu(dot(ffn, r.eg[...])) * dot(ffn, r.eu[...])).astype(BF16)
    shared_acts = []
    for c in range(2):
        both = dot_nt(ffn, r.shared[c, : 2 * units])
        shared_acts.append((silu(both[:, :units]) * both[:, units:]).astype(BF16))
    bg = r.bg[...].astype(F32).reshape(1, -1)
    branch = sigmoid(jnp.sum(ffn.astype(F32) * bg, axis=1, keepdims=True))
    weight = r.routed[:, 0:1]

    def target(s):
        return (2 * (s // group) + core) * group + lax.rem(s, group)

    def r_copy(s, q):
        return remote(
            r.rsend.at[s, q],
            r.rbuf.at[me * half + xi],
            r.rs.at[s, q],
            r.rr.at[me * half + xi],
            target(s),
            q,
        )

    def away(s, q):
        return jnp.logical_or(target(s) != me, q != tp)

    first = lax.rem(me, mates)
    for k in range(m):
        q = lax.rem(tp + k, m)
        at = pl.ds(pl.multiple_of(q * quarter, quarter), quarter)
        out = weight * dot(act, r.ed[:, at])
        side = dot(shared_acts[0], r.shared[0, 2 * units :, at])
        side = side + dot(shared_acts[1], r.shared[1, 2 * units :, at])
        r.rsend[:, q] = (out + branch * side).astype(BF16).reshape(mates, rows, quarter)

        def send_r(i, q=q):
            s = lax.rem(first + i, mates)

            @pl.when(away(s, q))
            def _():
                r_copy(s, q).start()

        loop(0, mates, send_r)

    @pl.when(held_here)
    def _():
        r.rbuf[me * half + xi] = r.rsend[place * group + which, tp]

    def got_r(i):
        p = lax.rem(me + i // half, n)
        a = lax.rem(xi + i, half)
        t = 2 * a + lax.rem(owner, 2)
        ref = r.rbuf.at[p * half + a]

        @pl.when(jnp.logical_or(p != me, t != tp))
        def _():
            remote(ref, ref, r.rs.at[0, 0], r.rr.at[p * half + a], p, t).wait_recv()

    loop(0, n * half, got_r)

    @pl.when(jnp.logical_not(held_here))
    def _():
        remote(r.rown, r.rown, r.ds.at[0], r.dr.at[0], me, pair).wait_recv()

    acc = jnp.concatenate([r.rown[b].astype(F32) for b in range(group)], axis=1)
    for p in range(n * half):
        acc = acc + r.rbuf[p].astype(F32)
    r.obuf[tp] = acc.astype(BF16)

    def o_copy(i):
        t = lax.rem(tp + i, m)
        return remote(r.obuf.at[tp], r.obuf.at[tp], r.os_.at[i], r.or_.at[tp], me, t)

    loop(1, m, lambda i: o_copy(i).start())

    def left_ep(i):
        x_copy(i).wait_send()
        s_copy(i).wait_send()
        a_copy(i).wait_send()
        b_copy(i).wait_send()
        f_copy(i).wait_send()
        for j in range(keys):
            h_copy(j, i).wait_send()

    loop(1, n, left_ep)

    def left_pass(i):
        s_pass(i).wait_send()
        for k in range(1, half):
            f_pass(i, k).wait_send()

    loop(0, n, left_pass)

    @pl.when(tp == me // group)
    def _():
        loop(1, n, lambda i: t_copy(i).wait_send())

    @pl.when(held_here)
    def _():
        d_copy().wait_send()

    for c in e_copies:
        c.wait_send()
    loop(1, m, lambda i: m_copy(i).wait_send())

    def left_r(i):
        s, q = i // m, lax.rem(i, m)

        @pl.when(away(s, q))
        def _():
            r_copy(s, q).wait_send()

    loop(0, mates * m, left_r)

    def got_o(i):
        t = lax.rem(tp + i, m)
        ref = r.obuf.at[t]
        remote(ref, ref, r.os_.at[i], r.or_.at[t], me, t).wait_recv()

    loop(1, m, got_o)
    for t in range(m):
        r.out[:, t * quarter : (t + 1) * quarter] = r.obuf[t]
    loop(1, m, lambda i: o_copy(i).wait_send())


def flush_kernel(layer_ref, state_ref, layer_out, state_out, sem):
    rows = state_ref.shape[0]
    part = rows // STATE_PARTS
    copies = [pltpu.make_async_copy(layer_ref, layer_out, sem.at[STATE_PARTS])]
    for i in range(STATE_PARTS):
        these = pl.ds(i * part, part)
        copies.append(
            pltpu.make_async_copy(state_ref.at[these], state_out.at[these], sem.at[i])
        )
    for c in copies:
        c.start()
    for c in copies:
        c.wait()


VMEM = pl.BlockSpec(memory_space=pltpu.VMEM)
HBM = pl.BlockSpec(memory_space=pltpu.HBM)


def per_device(
    n,
    m,
    tokens,
    norm_gain,
    query_weight,
    key_weight,
    value_weight,
    outgate_weight,
    beta_weight,
    decay_weight,
    decay_rate,
    decay_bias,
    head_gain,
    recurrent,
    output_weight,
    ffn_gain,
    routes,
    route_weight,
    expert_gate,
    expert_up,
    expert_down,
    shared_gate,
    shared_up,
    shared_down,
    branch_gate,
):
    rows, width = tokens.shape
    _, heads, key_dim, value_dim = recurrent.shape
    depth, qc = query_weight.shape
    vc = value_weight.shape[1]
    keys = qc // key_dim
    near = 2 * qc + vc
    half = m // 2
    group = n // m
    mates = half * group
    units = shared_gate.shape[1] // n
    cols = shared_down.shape[1]
    hidden = expert_gate.shape[2]
    quarter = width // m
    sds = jax.ShapeDtypeStruct
    dma = pltpu.SemaphoreType.DMA

    inputs = dict(
        tokens=tokens,
        gain=norm_gain,
        qw=query_weight,
        kw=key_weight,
        vw=value_weight,
        gw=outgate_weight,
        beta=beta_weight.T,
        decay=decay_weight.T,
        rate=decay_rate[None, :],
        bias=decay_bias[None, :],
        routes=routes.T,
        rw=route_weight.T,
        head_gain=head_gain,
        state=recurrent,
        ow=output_weight,
        ffn_gain=ffn_gain,
        eg=expert_gate,
        eu=expert_up,
        ed=expert_down,
        sg=shared_gate,
        su=shared_up,
        sd=shared_down,
        bg=branch_gate,
    )
    plain = ("tokens", "gain", "beta", "decay", "rate", "bias", "routes", "rw")
    plain += ("head_gain", "ffn_gain", "sg", "su", "sd", "bg", "ow")
    scratch = {k: pltpu.VMEM(inputs[k].shape, inputs[k].dtype) for k in plain}
    scratch.update(
        weights=pltpu.VMEM((depth, near + vc), BF16),
        eg=pltpu.VMEM((width, 2 * hidden), BF16),
        eu=pltpu.VMEM((width, 2 * hidden), BF16),
        ed=pltpu.VMEM((2 * hidden, width), BF16),
        xsend=pltpu.VMEM((n, rows, depth), BF16),
        xbuf=pltpu.VMEM((n, rows, depth), BF16),
        tsend=pltpu.VMEM((n, rows, depth), BF16),
        tbuf=pltpu.VMEM((group, rows, depth), BF16),
        ssend=pltpu.VMEM((n, 3 * units, cols), BF16),
        sbuf=pltpu.VMEM((2, n, 3 * units, cols), BF16),
        shared=pltpu.VMEM((2, 3 * units, width), BF16),
        asend=pltpu.VMEM((n, rows, near), BF16),
        abuf=pltpu.VMEM((n, rows, near), BF16),
        bsend=pltpu.VMEM((n, rows, vc + 128), BF16),
        bbuf=pltpu.VMEM((n, rows, vc + 128), BF16),
        retain=pltpu.VMEM((rows, vc), F32),
        pull=pltpu.VMEM((rows, vc), F32),
        push=pltpu.VMEM((rows, vc), F32),
        qk=pltpu.VMEM((rows, keys * value_dim), F32),
        kq=pltpu.VMEM((key_dim, 128), F32),
        held=pltpu.VMEM((rows, vc), F32),
        routed=pltpu.VMEM((mates * rows, 128), F32),
        hbuf=pltpu.VMEM((keys, n, rows, vc // keys), BF16),
        msend=pltpu.VMEM((m, group * rows, cols), BF16),
        mbuf=pltpu.VMEM((m, group * rows, cols), BF16),
        resid=pltpu.VMEM((half, n, group, rows, cols), BF16),
        rown=pltpu.VMEM((group, rows, cols), BF16),
        rsend=pltpu.VMEM((mates, m, rows, quarter), BF16),
        rbuf=pltpu.VMEM((n * half, rows, quarter), BF16),
        obuf=pltpu.VMEM((m, rows, quarter), BF16),
        wsem=dma((len(inputs) + STATE_PARTS,)),
        xs=dma((n,)),
        xr=dma((n,)),
        ss=dma((n,)),
        sr=dma((n,)),
        s2s=dma((n,)),
        s2r=dma((n,)),
        as_=dma((n,)),
        ar=dma((n,)),
        bs=dma((n,)),
        br=dma((n,)),
        ts=dma((n,)),
        tr=dma((group,)),
        hs=dma((keys, n)),
        hr=dma((keys, n)),
        ms=dma((m,)),
        mr=dma((m,)),
        fs=dma((n,)),
        fr=dma((n,)),
        gs=dma((half, n)),
        gr=dma((half, n)),
        es=dma((3,)),
        er=dma((3,)),
        ds=dma((1,)),
        dr=dma((1,)),
        rs=dma((mates, m)),
        rr=dma((n * half,)),
        os_=dma((m,)),
        or_=dma((m,)),
    )
    names = [k + "_hbm" for k in inputs] + ["out", "new"] + list(scratch)
    layer, state = pl.pallas_call(
        functools.partial(layer_kernel, n, m, names),
        out_shape=(pltpu.VMEM((rows, width), BF16), pltpu.VMEM(recurrent.shape, F32)),
        in_specs=[HBM] * len(inputs),
        out_specs=(VMEM, VMEM),
        scratch_shapes=list(scratch.values()),
        compiler_params=pltpu.CompilerParams(
            collective_id=0, has_side_effects=True, vmem_limit_bytes=48 * 2**20
        ),
    )(*(pltpu.with_memory_space_constraint(v, pltpu.HBM) for v in inputs.values()))

    return pl.pallas_call(
        flush_kernel,
        out_shape=(sds((rows, width), BF16), sds(recurrent.shape, F32)),
        in_specs=[VMEM, VMEM],
        out_specs=(HBM, HBM),
        scratch_shapes=[dma((STATE_PARTS + 1,))],
        compiler_params=pltpu.CompilerParams(vmem_limit_bytes=4 * 2**20),
    )(layer, state)


def solution(mesh):
    return jax.shard_map(
        functools.partial(per_device, mesh.shape["ep"], mesh.shape["tp"]),
        mesh=mesh,
        in_specs=(
            P("ep", None),
            P(),
            P("ep", "tp"),
            P("ep", "tp"),
            P("ep", "tp"),
            P("ep", "tp"),
            P(),
            P(),
            P("tp"),
            P("tp"),
            P(),
            P("ep", "tp", None, None),
            P("tp", "ep"),
            P(),
            P("ep", None),
            P("ep", None),
            P("ep", None, "tp"),
            P("ep", None, "tp"),
            P("ep", "tp", None),
            P("ep", "tp"),
            P("ep", "tp"),
            P("tp", "ep"),
            P(),
        ),
        out_specs=(P("ep", None), P("ep", "tp", None, None)),
        check_vma=False,
    )
```

time: 71.9 us -> 56.4 us (0.78)
  Pallas kernels: 69.4 us -> 55.6 us
  local copies, waits for them, and re-layouts: 1.47 us -> 0 us
    pallas_call x3 -> x2, Pallas kernels: 69.4 us -> 55.6 us  [the longest x1 53.5 us: per_device(): pl.pallas_call(functools.partial(layer_kernel, n, m, names), out_shape=(p...]
    unnamed x1 -> x0, local copies, waits for them, and re-layouts: 1.47 us -> none
where the time goes in v1:
time: 56.4 us; the launch traced here: 56.2 us
  Pallas kernels  55.6 us (99%)
  between operations  0.65 us (1%)
    pallas_call x1, Pallas kernels, per_device(): pl.pallas_call(functools.partial(layer_kernel, n, m, names), out_shape=(p...  53.5 us
    pallas_call x1, Pallas kernels, per_device(): pl.pallas_call(flush_kernel, out_shape=(sds((rows, width), BF16), sds(rec...  2.07 us

profile of v1, /device:TPU:0, one launch (start us, length us, event | category | flops | bytes accessed | tf_op | source)
XLA Modules:
  0.0 56.2 jit_solution(10025489816941193931)
XLA Ops:
  0.6 53.5 %shard_map.230 = (bf16[16,2048]{1,0:T(8,128)(2,1)S(1)}, f32[16,4,128,128]{3,2,1,0:T(8,128)S(1)}) custom-call(bf16[16,2048]{1,0:T(8,128)(2,1)} %refs_0_.1, bf16[2048]{0:T(1024)(128)(2,1)} %refs_1_.1, bf16[256,256]{1,0:T(8,128)(2,1)} %refs_2_.1, bf16[256,256]{1,0:T(8,128)(2,1)} %refs_3_.1, bf16[256,512]{1,0:T(8,128)(2,1)} %refs_4_.1, ...), custom_call_target="tpu_custom_call" | custom-call | tf_op jit(solution)/shard_map/pallas_call | solution.py:743
  54.2 2.1 %shard_map.231 = (bf16[16,2048]{1,0:T(8,128)(2,1)}, f32[16,4,128,128]{3,2,1,0:T(8,128)}) custom-call(bf16[16,2048]{1,0:T(8,128)(2,1)S(1)} %get-tuple-element.4.layer_ref, f32[16,4,128,128]{3,2,1,0:T(8,128)S(1)} %get-tuple-element.5.state_ref), custom_call_target="tpu_custom_call" | custom-call | tf_op jit(solution)/shard_map/pallas_call | solution.py:754

commit v2 on v1

v2 whole, which is shorter than its diff:
```python
import functools
import types

import jax
import jax.numpy as jnp
from jax import lax
from jax.experimental import pallas as pl
from jax.experimental.pallas import tpu as pltpu
from jax.sharding import PartitionSpec as P

EPS = 1e-06
ROUTED_SCALE = 2.5
MESH = pl.DeviceIdType.MESH
F32 = jnp.float32
BF16 = jnp.bfloat16
STATE_PARTS = 4


def silu(v):
    return v / (1.0 + jnp.exp(-v))


def sigmoid(v):
    return 1.0 / (1.0 + jnp.exp(-v))


def rms_scale(values, gain):
    values = values.astype(F32)
    return (
        values
        * lax.rsqrt(jnp.mean(values * values, axis=-1, keepdims=True) + EPS)
        * gain.astype(F32).reshape(1, -1)
    )


def unit_rows(values):
    return values * lax.rsqrt(jnp.sum(values * values, axis=-1, keepdims=True) + EPS)


def dot(a, b):
    return jnp.dot(a, b, preferred_element_type=F32)


def dot_nt(a, b):
    return lax.dot_general(a, b, (((1,), (1,)), ((), ())), preferred_element_type=F32)


def remote(src, dst, send_sem, recv_sem, e, t):
    return pltpu.make_async_remote_copy(
        src_ref=src,
        dst_ref=dst,
        send_sem=send_sem,
        recv_sem=recv_sem,
        device_id=(e, t),
        device_id_type=MESH,
    )


def loop(lo, hi, body):
    def step(i, c):
        body(i)
        return c

    lax.fori_loop(lo, hi, step, 0)


def layer_kernel(n, m, names, *refs):
    r = types.SimpleNamespace(**dict(zip(names, refs)))
    me, tp = lax.axis_index("ep"), lax.axis_index("tp")
    count = n * m
    lin = me * m + tp
    half = m // 2
    group = n // m
    core = lax.rem(tp, 2)
    pair = tp + 1 - 2 * core
    xi = tp // 2
    home = lax.rem(me, m)
    turn = me // m
    rows, width = r.tokens.shape
    depth, qc = r.qw_hbm.shape
    vc = r.vw_hbm.shape[1]
    key_dim, value_dim = r.new.shape[2], r.new.shape[3]
    heads = r.new.shape[1]
    keys = qc // key_dim
    share = heads // keys
    near = 2 * qc + vc
    cols = r.wide_ow.shape[1]
    hidden = r.eg_hbm.shape[2]
    quarter = width // m
    units = r.ssend2.shape[1]
    tall = group * rows

    barrier = pltpu.get_barrier_semaphore()

    def greet(i):
        p = lax.rem(lin + i, count)
        pl.semaphore_signal(
            barrier, inc=1, device_id=(p // m, lax.rem(p, m)), device_id_type=MESH
        )

    loop(1, count, greet)

    fetches, alone = {}, []

    def fetch(name, src, dst, sem=None):
        if sem is None:
            sem = r.wsem.at[len(alone)]
            alone.append(name)
        c = pltpu.make_async_copy(src, dst, sem)
        c.start()
        fetches[name] = c

    for name in ("tokens", "gain"):
        fetch(name, getattr(r, name + "_hbm"), getattr(r, name))
    at = 0
    for name in ("qw", "kw", "vw", "gw"):
        src = getattr(r, name + "_hbm")
        fetch(name, src, r.weights.at[:, pl.ds(at, src.shape[1])], r.psem.at[0])
        at += src.shape[1]
    for name in ("routes", "rw", "beta", "decay", "rate", "bias", "sg", "su", "sd"):
        fetch(name, getattr(r, name + "_hbm"), getattr(r, name))
    part = rows // STATE_PARTS
    for i in range(STATE_PARTS):
        these = pl.ds(i * part, part)
        fetch(("state", i), r.state_hbm.at[these], r.new.at[these], r.psem.at[1])
    for name in ("head_gain", "ffn_gain", "bg"):
        fetch(name, getattr(r, name + "_hbm"), getattr(r, name))
    own_ow = pl.ds(pl.multiple_of(tp * vc, vc), vc)
    mine = pl.ds(pl.multiple_of(core * hidden, hidden), hidden)
    other = pl.ds(pl.multiple_of((1 - core) * hidden, hidden), hidden)
    fetch("ow", r.ow_hbm, r.wide_ow.at[own_ow])
    fetch("eg", r.eg_hbm.at[0], r.eg.at[:, mine])
    fetch("eu", r.eu_hbm.at[0], r.eu.at[:, mine])
    fetch("ed", r.ed_hbm.at[0], r.ed.at[mine])

    steps = [
        (1 - 2 * lax.rem(me // 2**i, 2)) * 2**i for i in range(n.bit_length() - 1)
    ]

    def peer(k):
        p = me
        for i, step in enumerate(steps):
            if k >> i & 1:
                p = p + step
        return p

    cuts = (n // 2, 3 * n // 4, n), (n // 4, n // 2), (0, n // 4)
    spans = [cuts[0][:2], cuts[0][1:], cuts[1], cuts[2]]
    order = [k for lo, hi in spans for k in range(lo, hi) if k]

    def arrived(ref, sem):
        remote(ref, ref, sem, sem, me, pair).wait_recv()

    def left(ref, sem):
        remote(ref, ref, sem, sem, me, pair).wait_send()

    fetches["tokens"].wait()
    fetches["gain"].wait()
    tokens = r.tokens[...]
    normed = rms_scale(tokens, r.gain[...]).astype(BF16)
    for e in range(n):
        r.xsend[e] = normed[:, e * depth : (e + 1) * depth]
        r.tsend[e] = tokens[:, e * depth : (e + 1) * depth]

    fetches["routes"].wait()
    fetches["rw"].wait()
    rw = r.rw[...]
    scaled = rw / jnp.sum(rw, axis=0, keepdims=True) * ROUTED_SCALE
    routes = r.routes[...]
    expert = lax.broadcasted_iota(jnp.int32, (128, rows), 0)
    by_expert = jnp.zeros((128, rows), F32)
    for k in range(routes.shape[0]):
        by_expert = by_expert + jnp.where(
            expert == routes[k : k + 1, :], scaled[k : k + 1, :], 0.0
        )
    by_expert = by_expert.T
    lane = lax.broadcasted_iota(jnp.int32, (rows, 128), 1)
    for e in range(n):
        w = by_expert[:, e : e + 1]
        high = w.astype(BF16).astype(F32)
        r.csend[e] = jnp.where(lane < 64, high, w - high).astype(BF16)
    pl.semaphore_wait(barrier, count - 1)

    for g, (lo, hi) in enumerate(spans):
        for k in range(max(lo, 1), hi):
            p = peer(k)
            remote(r.xsend.at[p], r.xbuf.at[k], r.xs.at[0], r.xr.at[g], p, tp).start()
    r.xbuf[0] = r.xsend[me]
    for k in order:
        p = peer(k)
        remote(r.csend.at[p], r.cbuf.at[me], r.cs.at[0], r.cr.at[0], p, tp).start()
    r.cbuf[me] = r.csend[me]

    for i in range(1, m):
        t = lax.rem(tp + i, m)
        remote(r.ow_hbm, r.wide_ow.at[own_ow], r.ows.at[0], r.owr.at[0], me, t).start()
    e_copies = [
        remote(r.eg_hbm.at[0], r.eg.at[:, mine], r.es.at[0], r.er.at[0], me, pair),
        remote(r.eu_hbm.at[0], r.eu.at[:, mine], r.es.at[1], r.er.at[1], me, pair),
        remote(r.ed_hbm.at[0], r.ed.at[mine], r.es.at[2], r.er.at[2], me, pair),
    ]
    for c in e_copies:
        c.start()

    for name in ("beta", "decay", "rate", "bias", "sg", "su", "sd"):
        fetches[name].wait()
    column = lax.broadcasted_iota(jnp.int32, (rows, r.beta.shape[0]), 1)

    def own_heads(w):
        logits = dot_nt(normed, w)
        return [
            jnp.sum(jnp.where(column == tp * heads + h, logits, 0.0), axis=1, keepdims=True)
            for h in range(heads)
        ]

    def wide(v):
        return jnp.broadcast_to(v, (rows, value_dim))

    beta = own_heads(r.beta[...])
    decay = own_heads(r.decay[...])
    for h in range(heads):
        at = slice(h * value_dim, (h + 1) * value_dim)
        strength = sigmoid(wide(beta[h]))
        shifted = wide(decay[h]) + r.bias[:, h : h + 1]
        softplus = jnp.maximum(shifted, 0.0) + jnp.log1p(jnp.exp(-jnp.abs(shifted)))
        retain = jnp.exp(-r.rate[:, h : h + 1] * softplus)
        r.retain[:, at] = retain
        r.pull[:, at] = strength * retain
        r.push[:, at] = strength
    for at, name in enumerate(("sg", "su")):
        by_unit = getattr(r, name)[...].astype(F32).T.astype(BF16)
        for e in range(n):
            r.ssend1[e, at * units : (at + 1) * units] = by_unit[e * units : (e + 1) * units]
    for e in range(n):
        r.ssend2[e] = r.sd[e * units : (e + 1) * units]

    pltpu.make_async_copy(r.weights, r.weights, r.psem.at[0]).wait()
    for g, (lo, hi) in enumerate(spans):
        if hi > max(lo, 1):
            arrived(r.xbuf.at[pl.ds(max(lo, 1), hi - max(lo, 1))], r.xr.at[g])
        x = r.xbuf[lo:hi].reshape((hi - lo) * rows, depth)
        for c in range(0, near, 512):
            size = min(512, near - c)
            out = dot(x, r.weights[:, c : c + size])
            r.asend[lo:hi, :, c : c + size] = out.astype(BF16).reshape(hi - lo, rows, size)
        for k in range(max(lo, 1), hi):
            remote(
                r.asend.at[k], r.abuf.at[k], r.as_.at[0], r.ar.at[0], peer(k), tp
            ).start()
    r.abuf[0] = r.asend[0]
    x = r.xbuf[...].reshape(n * rows, depth)
    out = dot(x, r.weights[:, near:])
    r.bsend[...] = out.astype(BF16).reshape(n, rows, vc)
    for k in order:
        remote(r.bsend.at[k], r.bbuf.at[k], r.bs.at[0], r.br.at[0], peer(k), tp).start()
    r.bbuf[0] = r.bsend[0]

    at_home = tp == home

    @pl.when(at_home)
    def _():
        for k in order:
            p = peer(k)
            remote(
                r.tsend.at[p], r.tbuf.at[turn], r.ts.at[0], r.tr.at[0], p, tp
            ).start()
        r.tbuf[turn] = r.tsend[me]

    def send_shared(src, dst, s, d):
        for k in order:
            p = peer(k)
            remote(src.at[p], dst.at[core, me], s.at[0], d.at[0], p, tp).start()
        dst[core, me] = src[me]

    send_shared(r.ssend1, r.sbuf1, r.s1s, r.s1r)

    arrived(r.cbuf.at[pl.ds(0, n - 1)], r.cr.at[0])
    for a in range(half):
        for b in range(group):
            w = r.cbuf[b * m + 2 * a + core].astype(F32)
            r.routed[a, b * rows : (b + 1) * rows] = jnp.broadcast_to(
                w[:, 0:1] + w[:, 64:65], (rows, 128)
            )
    fetches["head_gain"].wait()
    pltpu.make_async_copy(r.new, r.new, r.psem.at[1]).wait()

    arrived(r.abuf.at[pl.ds(1, n - 1)], r.ar.at[0])

    def gathered(ref, c, size):
        acc = ref[0, :, c : c + size].astype(F32)
        for e in range(1, n):
            acc = acc + ref[e, :, c : c + size].astype(F32)
        return acc.astype(BF16).astype(F32)

    q_rows = [
        unit_rows(silu(gathered(r.abuf, j * key_dim, key_dim))) * key_dim ** (-0.5)
        for j in range(keys)
    ]
    k_rows = [
        unit_rows(silu(gathered(r.abuf, qc + j * key_dim, key_dim))) for j in range(keys)
    ]
    for h in range(heads):
        at = slice(h * value_dim, (h + 1) * value_dim)
        r.push[:, at] = r.push[:, at] * silu(
            gathered(r.abuf, 2 * qc + h * value_dim, value_dim)
        )
    for j in range(keys):
        r.qk[:, j * value_dim : (j + 1) * value_dim] = wide(
            jnp.sum(q_rows[j] * k_rows[j], axis=1, keepdims=True)
        )
    stacked = q_rows + k_rows
    stacked.append(jnp.zeros((128 - 2 * keys * rows, key_dim), F32))
    r.kq[...] = jnp.concatenate(stacked, axis=0).T

    for j in range(keys):
        for s in range(rows):
            q = jnp.broadcast_to(r.kq[:, j * rows + s : j * rows + s + 1], (key_dim, value_dim))
            at = (keys + j) * rows + s
            k = jnp.broadcast_to(r.kq[:, at : at + 1], (key_dim, value_dim))
            one = slice(s, s + 1)
            qk = r.qk[one, j * value_dim : (j + 1) * value_dim]
            for h in range(j * share, (j + 1) * share):
                c = slice(h * value_dim, (h + 1) * value_dim)
                state = r.new[s, h]
                retain = r.retain[one, c]
                predicted = jnp.sum(state * k, axis=0, keepdims=True)
                before = jnp.sum(state * q, axis=0, keepdims=True)
                correction = r.push[one, c] - r.pull[one, c] * predicted
                r.new[s, h] = state * retain + k * correction
                r.held[one, c] = before * retain + qk * correction

    arrived(r.bbuf.at[pl.ds(1, n - 1)], r.br.at[0])
    for h in range(heads):
        c = slice(h * value_dim, (h + 1) * value_dim)
        gate = silu(gathered(r.bbuf, h * value_dim, value_dim))
        r.hsend[:, c] = (rms_scale(r.held[:, c], r.head_gain[...]) * gate).astype(BF16)

    def send_h(p):
        remote(
            r.hsend, r.hbuf.at[turn * m + tp], r.hs.at[0], r.hr.at[0], p, home
        ).start()

    for k in order:
        send_h(peer(k))

    @pl.when(jnp.logical_not(at_home))
    def _():
        send_h(me)

    @pl.when(at_home)
    def _():
        r.hbuf[turn * m + tp] = r.hsend[...]

    send_shared(r.ssend2, r.sbuf2, r.s2s, r.s2r)

    fetches["ow"].wait()
    arrived(r.wide_ow.at[pl.ds(0, (m - 1) * vc)], r.owr.at[0])

    @pl.when(at_home)
    def _():
        arrived(r.tbuf.at[pl.ds(0, group - 1)], r.tr.at[0])
        arrived(r.hbuf.at[pl.ds(0, n - 1)], r.hr.at[0])

    @pl.when(jnp.logical_not(at_home))
    def _():
        arrived(r.tbuf, r.tr.at[0])
        arrived(r.hbuf, r.hr.at[0])

    residual = r.tbuf[...].reshape(tall, cols).astype(F32)
    mix = None
    for t in range(m):
        h = jnp.concatenate([r.hbuf[b * m + t] for b in range(group)], axis=0)
        term = dot(h, r.wide_ow[t * vc : (t + 1) * vc])
        mix = term if mix is None else mix + term
    r.resid[xi, me] = (residual + mix).astype(BF16).reshape(group, rows, cols)

    mine_resid = r.resid.at[xi, me]
    for k in order:
        remote(mine_resid, mine_resid, r.fs.at[0], r.fr.at[k], peer(k), tp).start()

    def f_pass(p):
        ref = r.resid.at[xi, p]
        for i in range(1, half):
            t = 2 * lax.rem(xi + i, half) + core
            remote(ref, ref, r.gs.at[0], r.gr.at[xi], me, t).start()

    f_pass(me)
    arrived(r.sbuf1.at[0, pl.ds(0, n - 1)], r.s1r.at[0])
    s_copies = [remote(r.sbuf1.at[core], r.sbuf1.at[core], r.ps.at[0], r.pr.at[0], me, pair)]
    s_copies[0].start()
    arrived(r.sbuf2.at[0, pl.ds(0, n - 1)], r.s2r.at[0])
    s_copies.append(
        remote(r.sbuf2.at[core], r.sbuf2.at[core], r.ps.at[1], r.pr.at[1], me, pair)
    )
    s_copies[1].start()
    for k in order:
        p = peer(k)
        arrived(r.resid.at[xi, p], r.fr.at[k])
        f_pass(p)
    arrived(r.sbuf1.at[0], r.pr.at[0])
    arrived(r.sbuf2.at[0], r.pr.at[1])
    for c in range(2):
        r.shared[c, : 2 * units] = jnp.concatenate([r.sbuf1[c, e] for e in range(n)], axis=1)
        r.shared[c, 2 * units :] = jnp.concatenate([r.sbuf2[c, e] for e in range(n)], axis=1)
    for name in ("ffn_gain", "bg", "eg", "eu", "ed"):
        fetches[name].wait()
    for i, ref in enumerate((r.eg.at[:, other], r.eu.at[:, other], r.ed.at[other])):
        arrived(ref, r.er.at[i])

    gain = r.ffn_gain[...].astype(F32).reshape(1, -1)
    bg = r.bg[...].astype(F32).reshape(1, -1)
    upper = me // (n // 2)

    def target(a, b):
        return b * m + 2 * a + core

    def away(a, b, q):
        return jnp.logical_or(target(a, b) != me, q != tp)

    def work(a):
        blocks = [r.resid[a, e].reshape(tall, cols).astype(F32) for e in range(n)]
        square = blocks[0] * blocks[0]
        for v in blocks[1:]:
            square = square + v * v
        scale = lax.rsqrt(jnp.sum(square, axis=1, keepdims=True) / width + EPS)
        ffn = jnp.concatenate(
            [
                (v * scale * gain[:, e * cols : (e + 1) * cols]).astype(BF16)
                for e, v in enumerate(blocks)
            ],
            axis=1,
        )
        act = (silu(dot(ffn, r.eg[...])) * dot(ffn, r.eu[...])).astype(BF16)
        dense = []
        for c in range(2):
            both = dot_nt(ffn, r.shared[c, : 2 * units])
            dense.append((silu(both[:, :units]) * both[:, units:]).astype(BF16))
        branch = sigmoid(jnp.sum(ffn.astype(F32) * bg, axis=1, keepdims=True))
        weight = r.routed[a, :, 0:1]
        for k in range(m):
            q = lax.rem(tp + k, m)
            at = pl.ds(pl.multiple_of(q * quarter, quarter), quarter)
            out = weight * dot(act, r.ed[:, at])
            side = dot(dense[0], r.shared[0, 2 * units :, at])
            side = side + dot(dense[1], r.shared[1, 2 * units :, at])
            r.rsend[a, :, q] = (out + branch * side).astype(BF16).reshape(group, rows, quarter)
            for i in range(group):
                b = lax.rem(i + (group // 2) * (1 - upper), group)

                @pl.when(away(a, b, q))
                def _():
                    remote(
                        r.rsend.at[a, b, q],
                        r.rbuf.at[me * half + xi],
                        r.rs.at[0],
                        r.rr.at[0],
                        target(a, b),
                        q,
                    ).start()

    work(xi)
    for i in range(1, half):
        a = lax.rem(xi + i, half)
        arrived(r.resid.at[a], r.gr.at[a])
        work(a)

    held_here = core == lax.rem(home, 2)
    place = home // 2
    d_copy = remote(
        r.resid.at[place, pl.ds(pair * group, group), turn],
        r.rown,
        r.ds.at[0],
        r.dr.at[0],
        me,
        pair,
    )

    @pl.when(held_here)
    def _():
        d_copy.start()
        r.rown[...] = r.resid[place, pl.ds(tp * group, group), turn]
        r.rbuf[me * half + xi] = r.rsend[place, turn, tp]

    left(r.xbuf.at[pl.ds(0, n - 1)], r.xs.at[0])
    left(r.cbuf.at[pl.ds(0, n - 1)], r.cs.at[0])
    left(r.abuf.at[pl.ds(0, n - 1)], r.as_.at[0])
    left(r.bbuf.at[pl.ds(0, n - 1)], r.bs.at[0])
    left(r.sbuf1.at[0, pl.ds(0, n - 1)], r.s1s.at[0])
    left(r.sbuf2.at[0, pl.ds(0, n - 1)], r.s2s.at[0])
    left(r.resid.at[0, pl.ds(0, n - 1)], r.fs.at[0])
    if half > 1:
        left(r.resid.at[pl.ds(0, half - 1)], r.gs.at[0])
    left(r.wide_ow.at[pl.ds(0, (m - 1) * vc)], r.ows.at[0])
    for c in e_copies + s_copies:
        c.wait_send()

    @pl.when(at_home)
    def _():
        left(r.tsend.at[pl.ds(0, n - 1)], r.ts.at[0])
        left(r.hbuf.at[pl.ds(0, n - 1)], r.hs.at[0])

    @pl.when(jnp.logical_not(at_home))
    def _():
        left(r.hbuf, r.hs.at[0])

    @pl.when(held_here)
    def _():
        arrived(r.rbuf.at[pl.ds(0, n * half - 1)], r.rr.at[0])

    @pl.when(jnp.logical_not(held_here))
    def _():
        arrived(r.rbuf, r.rr.at[0])
        arrived(r.rown, r.dr.at[0])

    acc = jnp.concatenate([r.rown[b].astype(F32) for b in range(group)], axis=1)
    for p in range(n * half):
        acc = acc + r.rbuf[p].astype(F32)
    r.obuf[tp] = acc.astype(BF16)
    for i in range(1, m):
        t = lax.rem(tp + i, m)
        remote(r.obuf.at[tp], r.obuf.at[tp], r.os_.at[0], r.or_.at[0], me, t).start()

    @pl.when(held_here)
    def _():
        d_copy.wait_send()
        left(r.rbuf.at[pl.ds(0, n * half - 1)], r.rs.at[0])

    @pl.when(jnp.logical_not(held_here))
    def _():
        left(r.rbuf, r.rs.at[0])

    arrived(r.obuf.at[pl.ds(0, m - 1)], r.or_.at[0])
    for t in range(m):
        r.out[:, t * quarter : (t + 1) * quarter] = r.obuf[t]
    left(r.obuf.at[pl.ds(0, m - 1)], r.os_.at[0])


def flush_kernel(layer_ref, state_ref, layer_out, state_out, sem):
    rows = state_ref.shape[0]
    part = rows // STATE_PARTS
    copies = [pltpu.make_async_copy(layer_ref, layer_out, sem.at[STATE_PARTS])]
    for i in range(STATE_PARTS):
        these = pl.ds(i * part, part)
        copies.append(
            pltpu.make_async_copy(state_ref.at[these], state_out.at[these], sem.at[i])
        )
    for c in copies:
        c.start()
    for c in copies:
        c.wait()


VMEM = pl.BlockSpec(memory_space=pltpu.VMEM)
HBM = pl.BlockSpec(memory_space=pltpu.HBM)


def per_device(
    n,
    m,
    tokens,
    norm_gain,
    query_weight,
    key_weight,
    value_weight,
    outgate_weight,
    beta_weight,
    decay_weight,
    decay_rate,
    decay_bias,
    head_gain,
    recurrent,
    output_weight,
    ffn_gain,
    routes,
    route_weight,
    expert_gate,
    expert_up,
    expert_down,
    shared_gate,
    shared_up,
    shared_down,
    branch_gate,
):
    rows, width = tokens.shape
    _, heads, key_dim, value_dim = recurrent.shape
    depth, qc = query_weight.shape
    vc = value_weight.shape[1]
    keys = qc // key_dim
    near = 2 * qc + vc
    half = m // 2
    group = n // m
    units = shared_gate.shape[1] // n
    cols = shared_down.shape[1]
    hidden = expert_gate.shape[2]
    quarter = width // m
    sds = jax.ShapeDtypeStruct
    dma = pltpu.SemaphoreType.DMA

    inputs = dict(
        tokens=tokens,
        gain=norm_gain,
        qw=query_weight,
        kw=key_weight,
        vw=value_weight,
        gw=outgate_weight,
        beta=beta_weight.T,
        decay=decay_weight.T,
        rate=decay_rate[None, :],
        bias=decay_bias[None, :],
        routes=routes.T,
        rw=route_weight.T,
        head_gain=head_gain,
        state=recurrent,
        ow=output_weight,
        ffn_gain=ffn_gain,
        eg=expert_gate,
        eu=expert_up,
        ed=expert_down,
        sg=shared_gate,
        su=shared_up,
        sd=shared_down,
        bg=branch_gate,
    )
    plain = ("tokens", "gain", "beta", "decay", "rate", "bias", "routes", "rw")
    plain += ("head_gain", "ffn_gain", "sg", "su", "sd", "bg")
    scratch = {k: pltpu.VMEM(inputs[k].shape, inputs[k].dtype) for k in plain}
    scratch.update(
        weights=pltpu.VMEM((depth, near + vc), BF16),
        wide_ow=pltpu.VMEM((m * vc, cols), BF16),
        eg=pltpu.VMEM((width, 2 * hidden), BF16),
        eu=pltpu.VMEM((width, 2 * hidden), BF16),
        ed=pltpu.VMEM((2 * hidden, width), BF16),
        xsend=pltpu.VMEM((n, rows, depth), BF16),
        xbuf=pltpu.VMEM((n, rows, depth), BF16),
        csend=pltpu.VMEM((n, rows, 128), BF16),
        cbuf=pltpu.VMEM((n, rows, 128), BF16),
        tsend=pltpu.VMEM((n, rows, depth), BF16),
        tbuf=pltpu.VMEM((group, rows, depth), BF16),
        ssend1=pltpu.VMEM((n, 2 * units, cols), BF16),
        sbuf1=pltpu.VMEM((2, n, 2 * units, cols), BF16),
        ssend2=pltpu.VMEM((n, units, cols), BF16),
        sbuf2=pltpu.VMEM((2, n, units, cols), BF16),
        shared=pltpu.VMEM((2, 3 * units, width), BF16),
        asend=pltpu.VMEM((n, rows, near), BF16),
        abuf=pltpu.VMEM((n, rows, near), BF16),
        bsend=pltpu.VMEM((n, rows, vc), BF16),
        bbuf=pltpu.VMEM((n, rows, vc), BF16),
        retain=pltpu.VMEM((rows, vc), F32),
        pull=pltpu.VMEM((rows, vc), F32),
        push=pltpu.VMEM((rows, vc), F32),
        qk=pltpu.VMEM((rows, keys * value_dim), F32),
        kq=pltpu.VMEM((key_dim, 128), F32),
        held=pltpu.VMEM((rows, vc), F32),
        routed=pltpu.VMEM((half, group * rows, 128), F32),
        hsend=pltpu.VMEM((rows, vc), BF16),
        hbuf=pltpu.VMEM((n, rows, vc), BF16),
        resid=pltpu.VMEM((half, n, group, rows, cols), BF16),
        rown=pltpu.VMEM((group, rows, cols), BF16),
        rsend=pltpu.VMEM((half, group, m, rows, quarter), BF16),
        rbuf=pltpu.VMEM((n * half, rows, quarter), BF16),
        obuf=pltpu.VMEM((m, rows, quarter), BF16),
        wsem=dma((len(inputs) - 5,)),
        psem=dma((2,)),
    )
    counts = dict(xr=4, fr=n, gr=half, es=3, er=3, ps=2, pr=2)
    for name in ("x", "c", "ow", "a", "b", "t", "s1", "s2", "h", "f", "g", "e", "p", "d", "r", "o"):
        for end in ("s", "r"):
            key = {"as": "as_", "os": "os_", "or": "or_"}.get(name + end, name + end)
            scratch[key] = dma((counts.get(key, 1),))
    names = [k + "_hbm" for k in inputs] + ["out", "new"] + list(scratch)
    layer, state = pl.pallas_call(
        functools.partial(layer_kernel, n, m, names),
        out_shape=(pltpu.VMEM((rows, width), BF16), pltpu.VMEM(recurrent.shape, F32)),
        in_specs=[HBM] * len(inputs),
        out_specs=(VMEM, VMEM),
        scratch_shapes=list(scratch.values()),
        compiler_params=pltpu.CompilerParams(
            collective_id=0, has_side_effects=True, vmem_limit_bytes=48 * 2**20
        ),
    )(*(pltpu.with_memory_space_constraint(v, pltpu.HBM) for v in inputs.values()))

    return pl.pallas_call(
        flush_kernel,
        out_shape=(sds((rows, width), BF16), sds(recurrent.shape, F32)),
        in_specs=[VMEM, VMEM],
        out_specs=(HBM, HBM),
        scratch_shapes=[dma((STATE_PARTS + 1,))],
        compiler_params=pltpu.CompilerParams(vmem_limit_bytes=4 * 2**20),
    )(layer, state)


def solution(mesh):
    return jax.shard_map(
        functools.partial(per_device, mesh.shape["ep"], mesh.shape["tp"]),
        mesh=mesh,
        in_specs=(
            P("ep", None),
            P(),
            P("ep", "tp"),
            P("ep", "tp"),
            P("ep", "tp"),
            P("ep", "tp"),
            P(),
            P(),
            P("tp"),
            P("tp"),
            P(),
            P("ep", "tp", None, None),
            P("tp", "ep"),
            P(),
            P("ep", None),
            P("ep", None),
            P("ep", None, "tp"),
            P("ep", None, "tp"),
            P("ep", "tp", None),
            P("ep", "tp"),
            P("ep", "tp"),
            P("tp", "ep"),
            P(),
        ),
        out_specs=(P("ep", None), P("ep", "tp", None, None)),
        check_vma=False,
    )
```

time: 56.4 us -> 49.4 us (0.88)
  Pallas kernels: 55.6 us -> 48.6 us
    pallas_call x1, Pallas kernels: 53.5 us -> 46.5 us  [per_device(): pl.pallas_call(functools.partial(layer_kernel, n, m, names), out_shape=(p...]
where the time goes in v2:
time: 49.4 us; the launch traced here: 49.2 us
  Pallas kernels  48.6 us (98%)
  between operations  0.65 us (1%)
    pallas_call x1, Pallas kernels, per_device(): pl.pallas_call(functools.partial(layer_kernel, n, m, names), out_shape=(p...  46.5 us
    pallas_call x1, Pallas kernels, per_device(): pl.pallas_call(flush_kernel, out_shape=(sds((rows, width), BF16), sds(rec...  2.07 us

profile of v2, /device:TPU:0, one launch (start us, length us, event | category | flops | bytes accessed | tf_op | source)
XLA Modules:
  0.0 49.2 jit_solution(7698626733169662537)
XLA Ops:
  0.6 46.5 %shard_map.230 = (bf16[16,2048]{1,0:T(8,128)(2,1)S(1)}, f32[16,4,128,128]{3,2,1,0:T(8,128)S(1)}) custom-call(bf16[16,2048]{1,0:T(8,128)(2,1)} %refs_0_.1, bf16[2048]{0:T(1024)(128)(2,1)} %refs_1_.1, bf16[256,256]{1,0:T(8,128)(2,1)} %refs_2_.1, bf16[256,256]{1,0:T(8,128)(2,1)} %refs_3_.1, bf16[256,512]{1,0:T(8,128)(2,1)} %refs_4_.1, ...), custom_call_target="tpu_custom_call" | custom-call | tf_op jit(solution)/shard_map/pallas_call | solution.py:671
  47.2 2.1 %shard_map.231 = (bf16[16,2048]{1,0:T(8,128)(2,1)}, f32[16,4,128,128]{3,2,1,0:T(8,128)}) custom-call(bf16[16,2048]{1,0:T(8,128)(2,1)S(1)} %get-tuple-element.4.layer_ref, f32[16,4,128,128]{3,2,1,0:T(8,128)S(1)} %get-tuple-element.5.state_ref), custom_call_target="tpu_custom_call" | custom-call | tf_op jit(solution)/shard_map/pallas_call | solution.py:682

commit v3 on v2

--- a/solution.py
+++ b/solution.py
@@ -67,8 +67,6 @@
 def layer_kernel(n, m, names, *refs):
     r = types.SimpleNamespace(**dict(zip(names, refs)))
     me, tp = lax.axis_index("ep"), lax.axis_index("tp")
-    count = n * m
-    lin = me * m + tp
     half = m // 2
     group = n // m
     core = lax.rem(tp, 2)
@@ -92,13 +90,27 @@
 
     barrier = pltpu.get_barrier_semaphore()
 
-    def greet(i):
-        p = lax.rem(lin + i, count)
+    steps = [
+        (1 - 2 * lax.rem(me // 2**i, 2)) * 2**i for i in range(n.bit_length() - 1)
+    ]
+
+    def peer(k):
+        p = me
+        for i, step in enumerate(steps):
+            if k >> i & 1:
+                p = p + step
+        return p
+
+    cuts = (n // 2, 3 * n // 4, n), (n // 4, n // 2), (0, n // 4)
+    spans = [cuts[0][:2], cuts[0][1:], cuts[1], cuts[2]]
+    order = [k for lo, hi in spans for k in range(lo, hi) if k]
+
+    for k in order:
+        pl.semaphore_signal(barrier, inc=1, device_id=(peer(k), tp), device_id_type=MESH)
+    for i in range(1, m):
         pl.semaphore_signal(
-            barrier, inc=1, device_id=(p // m, lax.rem(p, m)), device_id_type=MESH
+            barrier, inc=1, device_id=(me, lax.rem(tp + i, m)), device_id_type=MESH
         )
-
-    loop(1, count, greet)
 
     fetches, alone = {}, []
 
@@ -117,7 +129,7 @@
         src = getattr(r, name + "_hbm")
         fetch(name, src, r.weights.at[:, pl.ds(at, src.shape[1])], r.psem.at[0])
         at += src.shape[1]
-    for name in ("routes", "rw", "beta", "decay", "rate", "bias", "sg", "su", "sd"):
+    for name in ("routes", "rw", "sd", "beta", "decay", "rate", "bias", "sg", "su"):
         fetch(name, getattr(r, name + "_hbm"), getattr(r, name))
     part = rows // STATE_PARTS
     for i in range(STATE_PARTS):
@@ -132,21 +144,6 @@
     fetch("eg", r.eg_hbm.at[0], r.eg.at[:, mine])
     fetch("eu", r.eu_hbm.at[0], r.eu.at[:, mine])
     fetch("ed", r.ed_hbm.at[0], r.ed.at[mine])
-
-    steps = [
-        (1 - 2 * lax.rem(me // 2**i, 2)) * 2**i for i in range(n.bit_length() - 1)
-    ]
-
-    def peer(k):
-        p = me
-        for i, step in enumerate(steps):
-            if k >> i & 1:
-                p = p + step
-        return p
-
-    cuts = (n // 2, 3 * n // 4, n), (n // 4, n // 2), (0, n // 4)
-    spans = [cuts[0][:2], cuts[0][1:], cuts[1], cuts[2]]
-    order = [k for lo, hi in spans for k in range(lo, hi) if k]
 
     def arrived(ref, sem):
         remote(ref, ref, sem, sem, me, pair).wait_recv()
@@ -179,7 +176,10 @@
         w = by_expert[:, e : e + 1]
         high = w.astype(BF16).astype(F32)
         r.csend[e] = jnp.where(lane < 64, high, w - high).astype(BF16)
-    pl.semaphore_wait(barrier, count - 1)
+    fetches["sd"].wait()
+    for e in range(n):
+        r.ssend2[e] = r.sd[e * units : (e + 1) * units]
+    pl.semaphore_wait(barrier, n + m - 2)
 
     for g, (lo, hi) in enumerate(spans):
         for k in range(max(lo, 1), hi):
@@ -190,6 +190,14 @@
         p = peer(k)
         remote(r.csend.at[p], r.cbuf.at[me], r.cs.at[0], r.cr.at[0], p, tp).start()
     r.cbuf[me] = r.csend[me]
+
+    def send_shared(src, dst, s, d):
+        for k in order:
+            p = peer(k)
+            remote(src.at[p], dst.at[core, me], s.at[0], d.at[0], p, tp).start()
+        dst[core, me] = src[me]
+
+    send_shared(r.ssend2, r.sbuf2, r.s2s, r.s2r)
 
     for i in range(1, m):
         t = lax.rem(tp + i, m)
@@ -202,7 +210,7 @@
     for c in e_copies:
         c.start()
 
-    for name in ("beta", "decay", "rate", "bias", "sg", "su", "sd"):
+    for name in ("beta", "decay", "rate", "bias", "sg", "su"):
         fetches[name].wait()
     column = lax.broadcasted_iota(jnp.int32, (rows, r.beta.shape[0]), 1)
 
@@ -231,8 +239,6 @@
         by_unit = getattr(r, name)[...].astype(F32).T.astype(BF16)
         for e in range(n):
             r.ssend1[e, at * units : (at + 1) * units] = by_unit[e * units : (e + 1) * units]
-    for e in range(n):
-        r.ssend2[e] = r.sd[e * units : (e + 1) * units]
 
     pltpu.make_async_copy(r.weights, r.weights, r.psem.at[0]).wait()
     for g, (lo, hi) in enumerate(spans):
@@ -266,14 +272,6 @@
             ).start()
         r.tbuf[turn] = r.tsend[me]
 
-    def send_shared(src, dst, s, d):
-        for k in order:
-            p = peer(k)
-            remote(src.at[p], dst.at[core, me], s.at[0], d.at[0], p, tp).start()
-        dst[core, me] = src[me]
-
-    send_shared(r.ssend1, r.sbuf1, r.s1s, r.s1r)
-
     arrived(r.cbuf.at[pl.ds(0, n - 1)], r.cr.at[0])
     for a in range(half):
         for b in range(group):
@@ -351,7 +349,7 @@
     def _():
         r.hbuf[turn * m + tp] = r.hsend[...]
 
-    send_shared(r.ssend2, r.sbuf2, r.s2s, r.s2r)
+    send_shared(r.ssend1, r.sbuf1, r.s1s, r.s1r)
 
     fetches["ow"].wait()
     arrived(r.wide_ow.at[pl.ds(0, (m - 1) * vc)], r.owr.at[0])
@@ -393,7 +391,7 @@
         remote(r.sbuf2.at[core], r.sbuf2.at[core], r.ps.at[1], r.pr.at[1], me, pair)
     )
     s_copies[1].start()
-    for k in order:
+    for k in reversed(order):
         p = peer(k)
         arrived(r.resid.at[xi, p], r.fr.at[k])
         f_pass(p)

time: 49.4 us -> 47.5 us (0.962)
  Pallas kernels: 48.6 us -> 46.7 us
    pallas_call x1, Pallas kernels: 46.5 us -> 44.7 us  [per_device(): pl.pallas_call(functools.partial(layer_kernel, n, m, names), out_shape=(p...]
where the time goes in v3:
time: 47.5 us; the launch traced here: 47.4 us
  Pallas kernels  46.7 us (98%)
  between operations  0.65 us (1%)
    pallas_call x1, Pallas kernels, per_device(): pl.pallas_call(functools.partial(layer_kernel, n, m, names), out_shape=(p...  44.7 us
    pallas_call x1, Pallas kernels, per_device(): pl.pallas_call(flush_kernel, out_shape=(sds((rows, width), BF16), sds(rec...  2.07 us

profile of v3, /device:TPU:0, one launch (start us, length us, event | category | flops | bytes accessed | tf_op | source)
XLA Modules:
  0.0 47.4 jit_solution(8442837421270483217)
XLA Ops:
  0.6 44.7 %shard_map.230 = (bf16[16,2048]{1,0:T(8,128)(2,1)S(1)}, f32[16,4,128,128]{3,2,1,0:T(8,128)S(1)}) custom-call(bf16[16,2048]{1,0:T(8,128)(2,1)} %refs_0_.1, bf16[2048]{0:T(1024)(128)(2,1)} %refs_1_.1, bf16[256,256]{1,0:T(8,128)(2,1)} %refs_2_.1, bf16[256,256]{1,0:T(8,128)(2,1)} %refs_3_.1, bf16[256,512]{1,0:T(8,128)(2,1)} %refs_4_.1, ...), custom_call_target="tpu_custom_call" | custom-call | tf_op jit(solution)/shard_map/pallas_call | solution.py:669
  45.3 2.1 %shard_map.231 = (bf16[16,2048]{1,0:T(8,128)(2,1)}, f32[16,4,128,128]{3,2,1,0:T(8,128)}) custom-call(bf16[16,2048]{1,0:T(8,128)(2,1)S(1)} %get-tuple-element.4.layer_ref, f32[16,4,128,128]{3,2,1,0:T(8,128)S(1)} %get-tuple-element.5.state_ref), custom_call_target="tpu_custom_call" | custom-call | tf_op jit(solution)/shard_map/pallas_call | solution.py:680

commit v4 on v3

--- a/solution.py
+++ b/solution.py
@@ -141,8 +141,10 @@
     mine = pl.ds(pl.multiple_of(core * hidden, hidden), hidden)
     other = pl.ds(pl.multiple_of((1 - core) * hidden, hidden), hidden)
     fetch("ow", r.ow_hbm, r.wide_ow.at[own_ow])
-    fetch("eg", r.eg_hbm.at[0], r.eg.at[:, mine])
-    fetch("eu", r.eu_hbm.at[0], r.eu.at[:, mine])
+    mine_up = pl.ds(pl.multiple_of((2 + core) * hidden, hidden), hidden)
+    other_up = pl.ds(pl.multiple_of((3 - core) * hidden, hidden), hidden)
+    fetch("eg", r.eg_hbm.at[0], r.egu.at[:, mine])
+    fetch("eu", r.eu_hbm.at[0], r.egu.at[:, mine_up])
     fetch("ed", r.ed_hbm.at[0], r.ed.at[mine])
 
     def arrived(ref, sem):
@@ -186,11 +188,6 @@
             p = peer(k)
             remote(r.xsend.at[p], r.xbuf.at[k], r.xs.at[0], r.xr.at[g], p, tp).start()
     r.xbuf[0] = r.xsend[me]
-    for k in order:
-        p = peer(k)
-        remote(r.csend.at[p], r.cbuf.at[me], r.cs.at[0], r.cr.at[0], p, tp).start()
-    r.cbuf[me] = r.csend[me]
-
     def send_shared(src, dst, s, d):
         for k in order:
             p = peer(k)
@@ -203,8 +200,8 @@
         t = lax.rem(tp + i, m)
         remote(r.ow_hbm, r.wide_ow.at[own_ow], r.ows.at[0], r.owr.at[0], me, t).start()
     e_copies = [
-        remote(r.eg_hbm.at[0], r.eg.at[:, mine], r.es.at[0], r.er.at[0], me, pair),
-        remote(r.eu_hbm.at[0], r.eu.at[:, mine], r.es.at[1], r.er.at[1], me, pair),
+        remote(r.eg_hbm.at[0], r.egu.at[:, mine], r.es.at[0], r.er.at[0], me, pair),
+        remote(r.eu_hbm.at[0], r.egu.at[:, mine_up], r.es.at[1], r.er.at[1], me, pair),
         remote(r.ed_hbm.at[0], r.ed.at[mine], r.es.at[2], r.er.at[2], me, pair),
     ]
     for c in e_copies:
@@ -249,17 +246,33 @@
             size = min(512, near - c)
             out = dot(x, r.weights[:, c : c + size])
             r.asend[lo:hi, :, c : c + size] = out.astype(BF16).reshape(hi - lo, rows, size)
+        for k in range(lo + 1, hi, 2):
+            remote(
+                r.asend.at[k, :, pl.ds(2 * qc, vc)],
+                r.vpart.at[k // 2],
+                r.us.at[0],
+                r.ur.at[g],
+                peer(1),
+                tp,
+            ).start()
         for k in range(max(lo, 1), hi):
             remote(
-                r.asend.at[k], r.abuf.at[k], r.as_.at[0], r.ar.at[0], peer(k), tp
+                r.asend.at[k, :, pl.ds(0, 2 * qc)],
+                r.abuf.at[k],
+                r.as_.at[0],
+                r.ar.at[0],
+                peer(k),
+                tp,
             ).start()
-    r.abuf[0] = r.asend[0]
+    r.abuf[0] = r.asend[0, :, : 2 * qc]
     x = r.xbuf[...].reshape(n * rows, depth)
     out = dot(x, r.weights[:, near:])
     r.bsend[...] = out.astype(BF16).reshape(n, rows, vc)
     for k in order:
-        remote(r.bsend.at[k], r.bbuf.at[k], r.bs.at[0], r.br.at[0], peer(k), tp).start()
-    r.bbuf[0] = r.bsend[0]
+        if k % 2:
+            remote(
+                r.bsend.at[k], r.gpart.at[k // 2], r.ws.at[0], r.wr.at[0], peer(1), tp
+            ).start()
 
     at_home = tp == home
 
@@ -272,21 +285,39 @@
             ).start()
         r.tbuf[turn] = r.tsend[me]
 
-    arrived(r.cbuf.at[pl.ds(0, n - 1)], r.cr.at[0])
-    for a in range(half):
-        for b in range(group):
-            w = r.cbuf[b * m + 2 * a + core].astype(F32)
-            r.routed[a, b * rows : (b + 1) * rows] = jnp.broadcast_to(
-                w[:, 0:1] + w[:, 64:65], (rows, 128)
-            )
-    fetches["head_gain"].wait()
+    def send_on(k, own, part, src, dst, sent, got):
+        both = (own.astype(F32) + part[k].astype(F32)).astype(BF16)
+        if k == 0:
+            dst[0] = both
+        else:
+            src[k] = both
+            remote(src.at[k], dst.at[k], sent.at[0], got.at[0], peer(2 * k), tp).start()
+
+    for g, (lo, hi) in enumerate(spans):
+        arrived(r.vpart.at[pl.ds(lo // 2, (hi - lo) // 2)], r.ur.at[g])
+        for k in range(lo // 2, hi // 2):
+            own = r.asend[2 * k, :, 2 * qc :]
+            send_on(k, own, r.vpart, r.vsend, r.vbuf, r.vs, r.vr)
+    arrived(r.gpart, r.wr.at[0])
+    for lo, hi in spans:
+        for k in range(lo // 2, hi // 2):
+            send_on(k, r.bsend[2 * k], r.gpart, r.gsend, r.gbuf, r.bs, r.br)
+
+    for name in ("head_gain", "ffn_gain", "bg"):
+        fetches[name].wait()
+    gain = r.ffn_gain[...].astype(F32).reshape(1, -1)
+    bg = r.bg[...].astype(F32).reshape(1, -1)
+    for e in range(n):
+        r.gains[e] = gain[:, e * cols : (e + 1) * cols]
+        r.bgs[e] = bg[:, e * cols : (e + 1) * cols]
     pltpu.make_async_copy(r.new, r.new, r.psem.at[1]).wait()
 
     arrived(r.abuf.at[pl.ds(1, n - 1)], r.ar.at[0])
+    arrived(r.vbuf.at[pl.ds(1, n // 2 - 1)], r.vr.at[0])
 
     def gathered(ref, c, size):
         acc = ref[0, :, c : c + size].astype(F32)
-        for e in range(1, n):
+        for e in range(1, ref.shape[0]):
             acc = acc + ref[e, :, c : c + size].astype(F32)
         return acc.astype(BF16).astype(F32)
 
@@ -300,7 +331,7 @@
     for h in range(heads):
         at = slice(h * value_dim, (h + 1) * value_dim)
         r.push[:, at] = r.push[:, at] * silu(
-            gathered(r.abuf, 2 * qc + h * value_dim, value_dim)
+            gathered(r.vbuf, h * value_dim, value_dim)
         )
     for j in range(keys):
         r.qk[:, j * value_dim : (j + 1) * value_dim] = wide(
@@ -327,10 +358,10 @@
                 r.new[s, h] = state * retain + k * correction
                 r.held[one, c] = before * retain + qk * correction
 
-    arrived(r.bbuf.at[pl.ds(1, n - 1)], r.br.at[0])
+    arrived(r.gbuf.at[pl.ds(1, n // 2 - 1)], r.br.at[0])
     for h in range(heads):
         c = slice(h * value_dim, (h + 1) * value_dim)
-        gate = silu(gathered(r.bbuf, h * value_dim, value_dim))
+        gate = silu(gathered(r.gbuf, h * value_dim, value_dim))
         r.hsend[:, c] = (rms_scale(r.held[:, c], r.head_gain[...]) * gate).astype(BF16)
 
     def send_h(p):
@@ -350,6 +381,10 @@
         r.hbuf[turn * m + tp] = r.hsend[...]
 
     send_shared(r.ssend1, r.sbuf1, r.s1s, r.s1r)
+    for k in order:
+        p = peer(k)
+        remote(r.csend.at[p], r.cbuf.at[me], r.cs.at[0], r.cr.at[0], p, tp).start()
+    r.cbuf[me] = r.csend[me]
 
     fetches["ow"].wait()
     arrived(r.wide_ow.at[pl.ds(0, (m - 1) * vc)], r.owr.at[0])
@@ -376,13 +411,41 @@
     for k in order:
         remote(mine_resid, mine_resid, r.fs.at[0], r.fr.at[k], peer(k), tp).start()
 
-    def f_pass(p):
-        ref = r.resid.at[xi, p]
+    def f_pass(k):
+        ref = r.resid.at[xi, peer(k)]
+        sem = r.gr.at[xi, 2 * k // n]
         for i in range(1, half):
             t = 2 * lax.rem(xi + i, half) + core
-            remote(ref, ref, r.gs.at[0], r.gr.at[xi], me, t).start()
-
-    f_pass(me)
+            remote(ref, ref, r.gs.at[0], sem, me, t).start()
+
+    f_pass(0)
+
+    for name in ("eg", "eu", "ed"):
+        fetches[name].wait()
+    for i, ref in enumerate((r.egu.at[:, other], r.egu.at[:, other_up], r.ed.at[other])):
+        arrived(ref, r.er.at[i])
+
+    class Sums:
+        up = square = branch = 0.0
+        dense = [0.0, 0.0]
+
+    def scaled_block(a, p):
+        v = r.resid[a, p].reshape(tall, cols).astype(F32)
+        return v, (v * r.gains[p]).astype(BF16)
+
+    def absorb(sums, a, p):
+        v, u = scaled_block(a, p)
+        at = pl.ds(pl.multiple_of(p * cols, cols), cols)
+        sums.square = sums.square + v * v
+        sums.branch = sums.branch + u.astype(F32) * r.bgs[p]
+        sums.up = sums.up + dot(u, r.egu[at])
+
+    def absorb_dense(sums, a, p):
+        u = scaled_block(a, p)[1]
+        sums.dense = [d + dot_nt(u, r.sbuf1[c, p]) for c, d in enumerate(sums.dense)]
+
+    first = Sums()
+    absorb(first, xi, me)
     arrived(r.sbuf1.at[0, pl.ds(0, n - 1)], r.s1r.at[0])
     s_copies = [remote(r.sbuf1.at[core], r.sbuf1.at[core], r.ps.at[0], r.pr.at[0], me, pair)]
     s_copies[0].start()
@@ -391,22 +454,28 @@
         remote(r.sbuf2.at[core], r.sbuf2.at[core], r.ps.at[1], r.pr.at[1], me, pair)
     )
     s_copies[1].start()
-    for k in reversed(order):
-        p = peer(k)
-        arrived(r.resid.at[xi, p], r.fr.at[k])
-        f_pass(p)
+    for k in range(1, n // 2):
+        arrived(r.resid.at[xi, peer(k)], r.fr.at[k])
+        f_pass(k)
+        absorb(first, xi, peer(k))
     arrived(r.sbuf1.at[0], r.pr.at[0])
     arrived(r.sbuf2.at[0], r.pr.at[1])
     for c in range(2):
-        r.shared[c, : 2 * units] = jnp.concatenate([r.sbuf1[c, e] for e in range(n)], axis=1)
-        r.shared[c, 2 * units :] = jnp.concatenate([r.sbuf2[c, e] for e in range(n)], axis=1)
-    for name in ("ffn_gain", "bg", "eg", "eu", "ed"):
-        fetches[name].wait()
-    for i, ref in enumerate((r.eg.at[:, other], r.eu.at[:, other], r.ed.at[other])):
-        arrived(ref, r.er.at[i])
-
-    gain = r.ffn_gain[...].astype(F32).reshape(1, -1)
-    bg = r.bg[...].astype(F32).reshape(1, -1)
+        r.shared[c] = jnp.concatenate([r.sbuf2[c, e] for e in range(n)], axis=1)
+    for k in range(n // 2):
+        absorb_dense(first, xi, peer(k))
+    for k in range(n // 2, n):
+        arrived(r.resid.at[xi, peer(k)], r.fr.at[k])
+        f_pass(k)
+        absorb(first, xi, peer(k))
+        absorb_dense(first, xi, peer(k))
+    arrived(r.cbuf.at[pl.ds(0, n - 1)], r.cr.at[0])
+    for a in range(half):
+        for b in range(group):
+            w = r.cbuf[b * m + 2 * a + core].astype(F32)
+            r.routed[a, b * rows : (b + 1) * rows] = jnp.broadcast_to(
+                w[:, 0:1] + w[:, 64:65], (rows, 128)
+            )
     upper = me // (n // 2)
 
     def target(a, b):
@@ -415,32 +484,23 @@
     def away(a, b, q):
         return jnp.logical_or(target(a, b) != me, q != tp)
 
-    def work(a):
-        blocks = [r.resid[a, e].reshape(tall, cols).astype(F32) for e in range(n)]
-        square = blocks[0] * blocks[0]
-        for v in blocks[1:]:
-            square = square + v * v
-        scale = lax.rsqrt(jnp.sum(square, axis=1, keepdims=True) / width + EPS)
-        ffn = jnp.concatenate(
-            [
-                (v * scale * gain[:, e * cols : (e + 1) * cols]).astype(BF16)
-                for e, v in enumerate(blocks)
-            ],
-            axis=1,
-        )
-        act = (silu(dot(ffn, r.eg[...])) * dot(ffn, r.eu[...])).astype(BF16)
+    def finish(sums, a):
+        square = jnp.sum(sums.square, axis=1, keepdims=True)
+        scale = lax.rsqrt(square / width + EPS)
+        up = sums.up * scale
+        act = (silu(up[:, : 2 * hidden]) * up[:, 2 * hidden :]).astype(BF16)
         dense = []
-        for c in range(2):
-            both = dot_nt(ffn, r.shared[c, : 2 * units])
+        for d in sums.dense:
+            both = d * scale
             dense.append((silu(both[:, :units]) * both[:, units:]).astype(BF16))
-        branch = sigmoid(jnp.sum(ffn.astype(F32) * bg, axis=1, keepdims=True))
+        branch = sigmoid(jnp.sum(sums.branch, axis=1, keepdims=True) * scale)
         weight = r.routed[a, :, 0:1]
         for k in range(m):
-            q = lax.rem(tp + k, m)
+            q = 2 * lax.rem(xi + k // 2, half) + lax.rem(core + k, 2)
             at = pl.ds(pl.multiple_of(q * quarter, quarter), quarter)
             out = weight * dot(act, r.ed[:, at])
-            side = dot(dense[0], r.shared[0, 2 * units :, at])
-            side = side + dot(dense[1], r.shared[1, 2 * units :, at])
+            side = dot(dense[0], r.shared[0, :, at])
+            side = side + dot(dense[1], r.shared[1, :, at])
             r.rsend[a, :, q] = (out + branch * side).astype(BF16).reshape(group, rows, quarter)
             for i in range(group):
                 b = lax.rem(i + (group // 2) * (1 - upper), group)
@@ -456,11 +516,16 @@
                         q,
                     ).start()
 
-    work(xi)
+    finish(first, xi)
     for i in range(1, half):
         a = lax.rem(xi + i, half)
-        arrived(r.resid.at[a], r.gr.at[a])
-        work(a)
+        second = Sums()
+        for g in range(2):
+            arrived(r.resid.at[a, pl.ds(0, n // 2)], r.gr.at[a, g])
+            for k in range(g * n // 2, (g + 1) * n // 2):
+                absorb(second, a, peer(k))
+                absorb_dense(second, a, peer(k))
+        finish(second, a)
 
     held_here = core == lax.rem(home, 2)
     place = home // 2
@@ -482,7 +547,10 @@
     left(r.xbuf.at[pl.ds(0, n - 1)], r.xs.at[0])
     left(r.cbuf.at[pl.ds(0, n - 1)], r.cs.at[0])
     left(r.abuf.at[pl.ds(0, n - 1)], r.as_.at[0])
-    left(r.bbuf.at[pl.ds(0, n - 1)], r.bs.at[0])
+    left(r.vpart, r.us.at[0])
+    left(r.gpart, r.ws.at[0])
+    left(r.vbuf.at[pl.ds(0, n // 2 - 1)], r.vs.at[0])
+    left(r.gbuf.at[pl.ds(0, n // 2 - 1)], r.bs.at[0])
     left(r.sbuf1.at[0, pl.ds(0, n - 1)], r.s1s.at[0])
     left(r.sbuf2.at[0, pl.ds(0, n - 1)], r.s2s.at[0])
     left(r.resid.at[0, pl.ds(0, n - 1)], r.fs.at[0])
@@ -625,8 +693,9 @@
     scratch.update(
         weights=pltpu.VMEM((depth, near + vc), BF16),
         wide_ow=pltpu.VMEM((m * vc, cols), BF16),
-        eg=pltpu.VMEM((width, 2 * hidden), BF16),
-        eu=pltpu.VMEM((width, 2 * hidden), BF16),
+        egu=pltpu.VMEM((width, 4 * hidden), BF16),
+        gains=pltpu.VMEM((n, 1, cols), F32),
+        bgs=pltpu.VMEM((n, 1, cols), F32),
         ed=pltpu.VMEM((2 * hidden, width), BF16),
         xsend=pltpu.VMEM((n, rows, depth), BF16),
         xbuf=pltpu.VMEM((n, rows, depth), BF16),
@@ -638,11 +707,16 @@
         sbuf1=pltpu.VMEM((2, n, 2 * units, cols), BF16),
         ssend2=pltpu.VMEM((n, units, cols), BF16),
         sbuf2=pltpu.VMEM((2, n, units, cols), BF16),
-        shared=pltpu.VMEM((2, 3 * units, width), BF16),
+        shared=pltpu.VMEM((2, units, width), BF16),
         asend=pltpu.VMEM((n, rows, near), BF16),
-        abuf=pltpu.VMEM((n, rows, near), BF16),
+        abuf=pltpu.VMEM((n, rows, 2 * qc), BF16),
         bsend=pltpu.VMEM((n, rows, vc), BF16),
-        bbuf=pltpu.VMEM((n, rows, vc), BF16),
+        vpart=pltpu.VMEM((n // 2, rows, vc), BF16),
+        vsend=pltpu.VMEM((n // 2, rows, vc), BF16),
+        vbuf=pltpu.VMEM((n // 2, rows, vc), BF16),
+        gpart=pltpu.VMEM((n // 2, rows, vc), BF16),
+        gsend=pltpu.VMEM((n // 2, rows, vc), BF16),
+        gbuf=pltpu.VMEM((n // 2, rows, vc), BF16),
         retain=pltpu.VMEM((rows, vc), F32),
         pull=pltpu.VMEM((rows, vc), F32),
         push=pltpu.VMEM((rows, vc), F32),
@@ -660,11 +734,12 @@
         wsem=dma((len(inputs) - 5,)),
         psem=dma((2,)),
     )
-    counts = dict(xr=4, fr=n, gr=half, es=3, er=3, ps=2, pr=2)
-    for name in ("x", "c", "ow", "a", "b", "t", "s1", "s2", "h", "f", "g", "e", "p", "d", "r", "o"):
+    counts = dict(xr=4, ur=4, fr=n, es=3, er=3, ps=2, pr=2)
+    for name in ("x", "c", "ow", "a", "u", "w", "v", "b", "t", "s1", "s2", "h", "f", "g", "e", "p", "d", "r", "o"):
         for end in ("s", "r"):
             key = {"as": "as_", "os": "os_", "or": "or_"}.get(name + end, name + end)
             scratch[key] = dma((counts.get(key, 1),))
+    scratch["gr"] = dma((half, 2))
     names = [k + "_hbm" for k in inputs] + ["out", "new"] + list(scratch)
     layer, state = pl.pallas_call(
         functools.partial(layer_kernel, n, m, names),

time: 47.5 us -> 44.8 us (0.943)
  Pallas kernels: 46.7 us -> 44 us
    pallas_call x1, Pallas kernels: 44.7 us -> 41.9 us  [per_device(): pl.pallas_call(functools.partial(layer_kernel, n, m, names), out_shape=(p...]
where the time goes in v4:
time: 44.8 us; the launch traced here: 44.6 us
  Pallas kernels  44 us (98%)
  between operations  0.65 us (1%)
    pallas_call x1, Pallas kernels, per_device(): pl.pallas_call(functools.partial(layer_kernel, n, m, names), out_shape=(p...  41.9 us
    pallas_call x1, Pallas kernels, per_device(): pl.pallas_call(flush_kernel, out_shape=(sds((rows, width), BF16), sds(rec...  2.07 us

profile of v4, /device:TPU:0, one launch (start us, length us, event | category | flops | bytes accessed | tf_op | source)
XLA Modules:
  0.0 44.6 jit_solution(8212973398078585767)
XLA Ops:
  0.6 41.9 %shard_map.230 = (bf16[16,2048]{1,0:T(8,128)(2,1)S(1)}, f32[16,4,128,128]{3,2,1,0:T(8,128)S(1)}) custom-call(bf16[16,2048]{1,0:T(8,128)(2,1)} %refs_0_.1, bf16[2048]{0:T(1024)(128)(2,1)} %refs_1_.1, bf16[256,256]{1,0:T(8,128)(2,1)} %refs_2_.1, bf16[256,256]{1,0:T(8,128)(2,1)} %refs_3_.1, bf16[256,512]{1,0:T(8,128)(2,1)} %refs_4_.1, ...), custom_call_target="tpu_custom_call" | custom-call | tf_op jit(solution)/shard_map/pallas_call | solution.py:744
  42.6 2.1 %shard_map.231 = (bf16[16,2048]{1,0:T(8,128)(2,1)}, f32[16,4,128,128]{3,2,1,0:T(8,128)}) custom-call(bf16[16,2048]{1,0:T(8,128)(2,1)S(1)} %get-tuple-element.4.layer_ref, f32[16,4,128,128]{3,2,1,0:T(8,128)S(1)} %get-tuple-element.5.state_ref), custom_call_target="tpu_custom_call" | custom-call | tf_op jit(solution)/shard_map/pallas_call | solution.py:755

commit v5 on v4

--- a/solution.py
+++ b/solution.py
@@ -81,7 +81,7 @@
     heads = r.new.shape[1]
     keys = qc // key_dim
     share = heads // keys
-    near = 2 * qc + vc
+    total = 2 * qc + 2 * vc
     cols = r.wide_ow.shape[1]
     hidden = r.eg_hbm.shape[2]
     quarter = width // m
@@ -209,12 +209,12 @@
 
     for name in ("beta", "decay", "rate", "bias", "sg", "su"):
         fetches[name].wait()
-    column = lax.broadcasted_iota(jnp.int32, (rows, r.beta.shape[0]), 1)
+    place_of = lax.broadcasted_iota(jnp.int32, (rows, r.beta.shape[0]), 1)
 
     def own_heads(w):
         logits = dot_nt(normed, w)
         return [
-            jnp.sum(jnp.where(column == tp * heads + h, logits, 0.0), axis=1, keepdims=True)
+            jnp.sum(jnp.where(place_of == tp * heads + h, logits, 0.0), axis=1, keepdims=True)
             for h in range(heads)
         ]
 
@@ -242,14 +242,14 @@
         if hi > max(lo, 1):
             arrived(r.xbuf.at[pl.ds(max(lo, 1), hi - max(lo, 1))], r.xr.at[g])
         x = r.xbuf[lo:hi].reshape((hi - lo) * rows, depth)
-        for c in range(0, near, 512):
-            size = min(512, near - c)
+        for c in range(0, total, 512):
+            size = min(512, total - c)
             out = dot(x, r.weights[:, c : c + size])
             r.asend[lo:hi, :, c : c + size] = out.astype(BF16).reshape(hi - lo, rows, size)
         for k in range(lo + 1, hi, 2):
             remote(
-                r.asend.at[k, :, pl.ds(2 * qc, vc)],
-                r.vpart.at[k // 2],
+                r.asend.at[k, :, pl.ds(2 * qc, 2 * vc)],
+                r.part.at[k // 2],
                 r.us.at[0],
                 r.ur.at[g],
                 peer(1),
@@ -265,14 +265,6 @@
                 tp,
             ).start()
     r.abuf[0] = r.asend[0, :, : 2 * qc]
-    x = r.xbuf[...].reshape(n * rows, depth)
-    out = dot(x, r.weights[:, near:])
-    r.bsend[...] = out.astype(BF16).reshape(n, rows, vc)
-    for k in order:
-        if k % 2:
-            remote(
-                r.bsend.at[k], r.gpart.at[k // 2], r.ws.at[0], r.wr.at[0], peer(1), tp
-            ).start()
 
     at_home = tp == home
 
@@ -285,23 +277,18 @@
             ).start()
         r.tbuf[turn] = r.tsend[me]
 
-    def send_on(k, own, part, src, dst, sent, got):
-        both = (own.astype(F32) + part[k].astype(F32)).astype(BF16)
-        if k == 0:
-            dst[0] = both
-        else:
-            src[k] = both
-            remote(src.at[k], dst.at[k], sent.at[0], got.at[0], peer(2 * k), tp).start()
-
     for g, (lo, hi) in enumerate(spans):
-        arrived(r.vpart.at[pl.ds(lo // 2, (hi - lo) // 2)], r.ur.at[g])
+        arrived(r.part.at[pl.ds(lo // 2, (hi - lo) // 2)], r.ur.at[g])
         for k in range(lo // 2, hi // 2):
-            own = r.asend[2 * k, :, 2 * qc :]
-            send_on(k, own, r.vpart, r.vsend, r.vbuf, r.vs, r.vr)
-    arrived(r.gpart, r.wr.at[0])
-    for lo, hi in spans:
-        for k in range(lo // 2, hi // 2):
-            send_on(k, r.bsend[2 * k], r.gpart, r.gsend, r.gbuf, r.bs, r.br)
+            own = r.asend[2 * k, :, 2 * qc :].astype(F32)
+            both = (own + r.part[k].astype(F32)).astype(BF16)
+            if k == 0:
+                r.vbuf[0] = both
+            else:
+                r.vsend[k] = both
+                remote(
+                    r.vsend.at[k], r.vbuf.at[k], r.vs.at[0], r.vr.at[0], peer(2 * k), tp
+                ).start()
 
     for name in ("head_gain", "ffn_gain", "bg"):
         fetches[name].wait()
@@ -313,7 +300,6 @@
     pltpu.make_async_copy(r.new, r.new, r.psem.at[1]).wait()
 
     arrived(r.abuf.at[pl.ds(1, n - 1)], r.ar.at[0])
-    arrived(r.vbuf.at[pl.ds(1, n // 2 - 1)], r.vr.at[0])
 
     def gathered(ref, c, size):
         acc = ref[0, :, c : c + size].astype(F32)
@@ -328,11 +314,6 @@
     k_rows = [
         unit_rows(silu(gathered(r.abuf, qc + j * key_dim, key_dim))) for j in range(keys)
     ]
-    for h in range(heads):
-        at = slice(h * value_dim, (h + 1) * value_dim)
-        r.push[:, at] = r.push[:, at] * silu(
-            gathered(r.vbuf, h * value_dim, value_dim)
-        )
     for j in range(keys):
         r.qk[:, j * value_dim : (j + 1) * value_dim] = wide(
             jnp.sum(q_rows[j] * k_rows[j], axis=1, keepdims=True)
@@ -341,28 +322,29 @@
     stacked.append(jnp.zeros((128 - 2 * keys * rows, key_dim), F32))
     r.kq[...] = jnp.concatenate(stacked, axis=0).T
 
+    def column(at):
+        return jnp.broadcast_to(r.kq[:, at : at + 1], (key_dim, value_dim))
+
     for j in range(keys):
         for s in range(rows):
-            q = jnp.broadcast_to(r.kq[:, j * rows + s : j * rows + s + 1], (key_dim, value_dim))
-            at = (keys + j) * rows + s
-            k = jnp.broadcast_to(r.kq[:, at : at + 1], (key_dim, value_dim))
-            one = slice(s, s + 1)
-            qk = r.qk[one, j * value_dim : (j + 1) * value_dim]
+            q, k = column(j * rows + s), column((keys + j) * rows + s)
             for h in range(j * share, (j + 1) * share):
                 c = slice(h * value_dim, (h + 1) * value_dim)
                 state = r.new[s, h]
-                retain = r.retain[one, c]
-                predicted = jnp.sum(state * k, axis=0, keepdims=True)
-                before = jnp.sum(state * q, axis=0, keepdims=True)
-                correction = r.push[one, c] - r.pull[one, c] * predicted
-                r.new[s, h] = state * retain + k * correction
-                r.held[one, c] = before * retain + qk * correction
-
-    arrived(r.gbuf.at[pl.ds(1, n // 2 - 1)], r.br.at[0])
+                r.seen[s : s + 1, c] = jnp.sum(state * k, axis=0, keepdims=True)
+                r.held[s : s + 1, c] = jnp.sum(state * q, axis=0, keepdims=True)
+
+    arrived(r.vbuf.at[pl.ds(1, n // 2 - 1)], r.vr.at[0])
     for h in range(heads):
         c = slice(h * value_dim, (h + 1) * value_dim)
-        gate = silu(gathered(r.gbuf, h * value_dim, value_dim))
-        r.hsend[:, c] = (rms_scale(r.held[:, c], r.head_gain[...]) * gate).astype(BF16)
+        j = h // share
+        values = silu(gathered(r.vbuf, h * value_dim, value_dim))
+        gate = silu(gathered(r.vbuf, vc + h * value_dim, value_dim))
+        correction = r.push[:, c] * values - r.pull[:, c] * r.seen[:, c]
+        r.seen[:, c] = correction
+        qk = r.qk[:, j * value_dim : (j + 1) * value_dim]
+        readout = r.held[:, c] * r.retain[:, c] + qk * correction
+        r.hsend[:, c] = (rms_scale(readout, r.head_gain[...]) * gate).astype(BF16)
 
     def send_h(p):
         remote(
@@ -385,6 +367,15 @@
         p = peer(k)
         remote(r.csend.at[p], r.cbuf.at[me], r.cs.at[0], r.cr.at[0], p, tp).start()
     r.cbuf[me] = r.csend[me]
+
+    for j in range(keys):
+        for s in range(rows):
+            k = column((keys + j) * rows + s)
+            for h in range(j * share, (j + 1) * share):
+                c = slice(h * value_dim, (h + 1) * value_dim)
+                r.new[s, h] = (
+                    r.new[s, h] * r.retain[s : s + 1, c] + k * r.seen[s : s + 1, c]
+                )
 
     fetches["ow"].wait()
     arrived(r.wide_ow.at[pl.ds(0, (m - 1) * vc)], r.owr.at[0])
@@ -547,10 +538,8 @@
     left(r.xbuf.at[pl.ds(0, n - 1)], r.xs.at[0])
     left(r.cbuf.at[pl.ds(0, n - 1)], r.cs.at[0])
     left(r.abuf.at[pl.ds(0, n - 1)], r.as_.at[0])
-    left(r.vpart, r.us.at[0])
-    left(r.gpart, r.ws.at[0])
+    left(r.part, r.us.at[0])
     left(r.vbuf.at[pl.ds(0, n // 2 - 1)], r.vs.at[0])
-    left(r.gbuf.at[pl.ds(0, n // 2 - 1)], r.bs.at[0])
     left(r.sbuf1.at[0, pl.ds(0, n - 1)], r.s1s.at[0])
     left(r.sbuf2.at[0, pl.ds(0, n - 1)], r.s2s.at[0])
     left(r.resid.at[0, pl.ds(0, n - 1)], r.fs.at[0])
@@ -652,7 +641,7 @@
     depth, qc = query_weight.shape
     vc = value_weight.shape[1]
     keys = qc // key_dim
-    near = 2 * qc + vc
+    total = 2 * qc + 2 * vc
     half = m // 2
     group = n // m
     units = shared_gate.shape[1] // n
@@ -691,7 +680,7 @@
     plain += ("head_gain", "ffn_gain", "sg", "su", "sd", "bg")
     scratch = {k: pltpu.VMEM(inputs[k].shape, inputs[k].dtype) for k in plain}
     scratch.update(
-        weights=pltpu.VMEM((depth, near + vc), BF16),
+        weights=pltpu.VMEM((depth, total), BF16),
         wide_ow=pltpu.VMEM((m * vc, cols), BF16),
         egu=pltpu.VMEM((width, 4 * hidden), BF16),
         gains=pltpu.VMEM((n, 1, cols), F32),
@@ -708,15 +697,12 @@
         ssend2=pltpu.VMEM((n, units, cols), BF16),
         sbuf2=pltpu.VMEM((2, n, units, cols), BF16),
         shared=pltpu.VMEM((2, units, width), BF16),
-        asend=pltpu.VMEM((n, rows, near), BF16),
+        asend=pltpu.VMEM((n, rows, total), BF16),
         abuf=pltpu.VMEM((n, rows, 2 * qc), BF16),
-        bsend=pltpu.VMEM((n, rows, vc), BF16),
-        vpart=pltpu.VMEM((n // 2, rows, vc), BF16),
-        vsend=pltpu.VMEM((n // 2, rows, vc), BF16),
-        vbuf=pltpu.VMEM((n // 2, rows, vc), BF16),
-        gpart=pltpu.VMEM((n // 2, rows, vc), BF16),
-        gsend=pltpu.VMEM((n // 2, rows, vc), BF16),
-        gbuf=pltpu.VMEM((n // 2, rows, vc), BF16),
+        part=pltpu.VMEM((n // 2, rows, 2 * vc), BF16),
+        vsend=pltpu.VMEM((n // 2, rows, 2 * vc), BF16),
+        vbuf=pltpu.VMEM((n // 2, rows, 2 * vc), BF16),
+        seen=pltpu.VMEM((rows, vc), F32),
         retain=pltpu.VMEM((rows, vc), F32),
         pull=pltpu.VMEM((rows, vc), F32),
         push=pltpu.VMEM((rows, vc), F32),
@@ -735,7 +721,7 @@
         psem=dma((2,)),
     )
     counts = dict(xr=4, ur=4, fr=n, es=3, er=3, ps=2, pr=2)
-    for name in ("x", "c", "ow", "a", "u", "w", "v", "b", "t", "s1", "s2", "h", "f", "g", "e", "p", "d", "r", "o"):
+    for name in ("x", "c", "ow", "a", "u", "v", "t", "s1", "s2", "h", "f", "g", "e", "p", "d", "r", "o"):
         for end in ("s", "r"):
             key = {"as": "as_", "os": "os_", "or": "or_"}.get(name + end, name + end)
             scratch[key] = dma((counts.get(key, 1),))

time: 44.8 us -> 43.9 us (0.980)
  Pallas kernels: 44 us -> 43.1 us
    pallas_call x1, Pallas kernels: 41.9 us -> 41.1 us  [per_device(): pl.pallas_call(functools.partial(layer_kernel, n, m, names), out_shape=(p...]
where the time goes in v5:
time: 43.9 us; the launch traced here: 43.8 us
  Pallas kernels  43.1 us (98%)
  between operations  0.65 us (1%)
    pallas_call x1, Pallas kernels, per_device(): pl.pallas_call(functools.partial(layer_kernel, n, m, names), out_shape=(p...  41.1 us
    pallas_call x1, Pallas kernels, per_device(): pl.pallas_call(flush_kernel, out_shape=(sds((rows, width), BF16), sds(rec...  2.07 us

profile of v5, /device:TPU:0, one launch (start us, length us, event | category | flops | bytes accessed | tf_op | source)
XLA Modules:
  0.0 43.8 jit_solution(12395904676972097428)
XLA Ops:
  0.6 41.1 %shard_map.230 = (bf16[16,2048]{1,0:T(8,128)(2,1)S(1)}, f32[16,4,128,128]{3,2,1,0:T(8,128)S(1)}) custom-call(bf16[16,2048]{1,0:T(8,128)(2,1)} %refs_0_.1, bf16[2048]{0:T(1024)(128)(2,1)} %refs_1_.1, bf16[256,256]{1,0:T(8,128)(2,1)} %refs_2_.1, bf16[256,256]{1,0:T(8,128)(2,1)} %refs_3_.1, bf16[256,512]{1,0:T(8,128)(2,1)} %refs_4_.1, ...), custom_call_target="tpu_custom_call" | custom-call | tf_op jit(solution)/shard_map/pallas_call | solution.py:730
  41.7 2.1 %shard_map.231 = (bf16[16,2048]{1,0:T(8,128)(2,1)}, f32[16,4,128,128]{3,2,1,0:T(8,128)}) custom-call(bf16[16,2048]{1,0:T(8,128)(2,1)S(1)} %get-tuple-element.4.layer_ref, f32[16,4,128,128]{3,2,1,0:T(8,128)S(1)} %get-tuple-element.5.state_ref), custom_call_target="tpu_custom_call" | custom-call | tf_op jit(solution)/shard_map/pallas_call | solution.py:741

commit v6 on v5

--- a/solution.py
+++ b/solution.py
@@ -238,7 +238,7 @@
             r.ssend1[e, at * units : (at + 1) * units] = by_unit[e * units : (e + 1) * units]
 
     pltpu.make_async_copy(r.weights, r.weights, r.psem.at[0]).wait()
-    for g, (lo, hi) in enumerate(spans):
+    for g, (lo, hi) in reversed(list(enumerate(spans))):
         if hi > max(lo, 1):
             arrived(r.xbuf.at[pl.ds(max(lo, 1), hi - max(lo, 1))], r.xr.at[g])
         x = r.xbuf[lo:hi].reshape((hi - lo) * rows, depth)
@@ -277,7 +277,7 @@
             ).start()
         r.tbuf[turn] = r.tsend[me]
 
-    for g, (lo, hi) in enumerate(spans):
+    for g, (lo, hi) in reversed(list(enumerate(spans))):
         arrived(r.part.at[pl.ds(lo // 2, (hi - lo) // 2)], r.ur.at[g])
         for k in range(lo // 2, hi // 2):
             own = r.asend[2 * k, :, 2 * qc :].astype(F32)
@@ -348,7 +348,7 @@
 
     def send_h(p):
         remote(
-            r.hsend, r.hbuf.at[turn * m + tp], r.hs.at[0], r.hr.at[0], p, home
+            r.hsend, r.hbuf.at[turn * m + tp], r.hs.at[0], r.hr.at[tp], p, home
         ).start()
 
     for k in order:
@@ -383,18 +383,21 @@
     @pl.when(at_home)
     def _():
         arrived(r.tbuf.at[pl.ds(0, group - 1)], r.tr.at[0])
-        arrived(r.hbuf.at[pl.ds(0, n - 1)], r.hr.at[0])
+        arrived(r.hbuf.at[pl.ds(0, group - 1)], r.hr.at[tp])
 
     @pl.when(jnp.logical_not(at_home))
     def _():
         arrived(r.tbuf, r.tr.at[0])
-        arrived(r.hbuf, r.hr.at[0])
+        arrived(r.hbuf.at[pl.ds(0, group)], r.hr.at[tp])
 
     residual = r.tbuf[...].reshape(tall, cols).astype(F32)
     mix = None
-    for t in range(m):
+    for i in range(m):
+        t = 2 * lax.rem(xi + i // 2, half) + lax.rem(core + i, 2)
+        if i:
+            arrived(r.hbuf.at[pl.ds(0, group)], r.hr.at[t])
         h = jnp.concatenate([r.hbuf[b * m + t] for b in range(group)], axis=0)
-        term = dot(h, r.wide_ow[t * vc : (t + 1) * vc])
+        term = dot(h, r.wide_ow[pl.ds(pl.multiple_of(t * vc, vc), vc)])
         mix = term if mix is None else mix + term
     r.resid[xi, me] = (residual + mix).astype(BF16).reshape(group, rows, cols)
 
@@ -720,7 +723,7 @@
         wsem=dma((len(inputs) - 5,)),
         psem=dma((2,)),
     )
-    counts = dict(xr=4, ur=4, fr=n, es=3, er=3, ps=2, pr=2)
+    counts = dict(xr=4, hr=m, ur=4, fr=n, es=3, er=3, ps=2, pr=2)
     for name in ("x", "c", "ow", "a", "u", "v", "t", "s1", "s2", "h", "f", "g", "e", "p", "d", "r", "o"):
         for end in ("s", "r"):
             key = {"as": "as_", "os": "os_", "or": "or_"}.get(name + end, name + end)

time: 43.9 us -> 43.3 us (0.986)
  Pallas kernels: 43.1 us -> 42.5 us
    pallas_call x1, Pallas kernels: 41.1 us -> 40.4 us  [per_device(): pl.pallas_call(functools.partial(layer_kernel, n, m, names), out_shape=(p...]
where the time goes in v6:
time: 43.3 us; the launch traced here: 43.1 us
  Pallas kernels  42.5 us (98%)
  between operations  0.65 us (2%)
    pallas_call x1, Pallas kernels, per_device(): pl.pallas_call(functools.partial(layer_kernel, n, m, names), out_shape=(p...  40.4 us
    pallas_call x1, Pallas kernels, per_device(): pl.pallas_call(flush_kernel, out_shape=(sds((rows, width), BF16), sds(rec...  2.07 us

profile of v6, /device:TPU:0, one launch (start us, length us, event | category | flops | bytes accessed | tf_op | source)
XLA Modules:
  0.0 43.1 jit_solution(335290968829897431)
XLA Ops:
  0.6 40.4 %shard_map.230 = (bf16[16,2048]{1,0:T(8,128)(2,1)S(1)}, f32[16,4,128,128]{3,2,1,0:T(8,128)S(1)}) custom-call(bf16[16,2048]{1,0:T(8,128)(2,1)} %refs_0_.1, bf16[2048]{0:T(1024)(128)(2,1)} %refs_1_.1, bf16[256,256]{1,0:T(8,128)(2,1)} %refs_2_.1, bf16[256,256]{1,0:T(8,128)(2,1)} %refs_3_.1, bf16[256,512]{1,0:T(8,128)(2,1)} %refs_4_.1, ...), custom_call_target="tpu_custom_call" | custom-call | tf_op jit(solution)/shard_map/pallas_call | solution.py:733
  41.1 2.1 %shard_map.231 = (bf16[16,2048]{1,0:T(8,128)(2,1)}, f32[16,4,128,128]{3,2,1,0:T(8,128)}) custom-call(bf16[16,2048]{1,0:T(8,128)(2,1)S(1)} %get-tuple-element.4.layer_ref, f32[16,4,128,128]{3,2,1,0:T(8,128)S(1)} %get-tuple-element.5.state_ref), custom_call_target="tpu_custom_call" | custom-call | tf_op jit(solution)/shard_map/pallas_call | solution.py:744
